TPU v7x, 256 devices: a 4x2x16 block of a 4x16x16 slice. The times are simulated.
256 devices in a mesh: grp: 2 (over y), st: 32 (over z, core), tp: 4 (over x).
Axes of the slice: x: 4, y: 2, z: 16, core: 2. Of those that a mesh axis runs over, the one named last changes fastest.
The devices are a block of a 4x16x16 slice.
Arguments:
- tokens: bfloat16 [32768, 2048], P(('grp', 'st'), 'tp'), parts along dimension 0, may hold values from -180 to 180
- ret_query: bfloat16 [32768, 1024], P(('grp', 'st'), 'tp'), parts along dimension 0, may hold values from -6 to 6
- ret_key: bfloat16 [32768, 1024], P(('grp', 'st'), 'tp'), parts along dimension 0, may hold values from -6 to 6
- ret_value: bfloat16 [32768, 1024], P(('grp', 'st'), 'tp'), parts along dimension 0, may hold values from -6 to 6
- w_query: bfloat16 [2048, 2048], P(None, 'tp'), may hold values from -0.125 to 0.125
- w_key: bfloat16 [2048, 2048], P(None, 'tp'), may hold values from -0.125 to 0.125
- w_value: bfloat16 [2048, 2048], P(None, 'tp'), may hold values from -0.125 to 0.125
- w_gate: bfloat16 [2048, 4], replicated, may hold values from -0.125 to 0.125
- store: bfloat16 [192, 128, 2048], P('st'), may hold values from -6 to 6
- passage_ids: int32 [512, 4], P(('grp', 'st')), parts along dimension 0, may hold values from 0 to 191, as said below
Outputs:
- blended: bfloat16 [32768, 3072], P(('grp', 'st'), 'tp'), parts along dimension 0
There are 2 independent parts, one for each index of `grp`. A program takes and returns all parts, laid end to end along the dimension named above; an argument that names none is the same for every part. Nothing has to cross between parts.
Inputs may be any that keep to these rules, and one draw needn't show every extreme that they name: `passage_ids`: passage p lies on index p // 6 of st. The 8 rows of one device name passages of any one index of st at most 2 times in all, and those of some index exactly 2 times.
All inputs are finite; a program needn't handle non-finite values.
Results may differ from a plain program's by a relative error of at most 0.0094.
Values may be sent and summed in bfloat16 or wider, within the bound.
A program may use at most 128 MiB of HBM per device.

v0:
```python
import jax
import jax.numpy as jnp
from jax import lax
from jax.sharding import PartitionSpec as P

RET_DIM = 256
HEAD_DIM = 512
BLOCK = 64
NPB = 4
SEQ_LEN = 256


ROTARY_BASE = 10000.0
NORM_EPS = 1e-05


def joined_along(pieces, dim):
    lengths = list(pieces.shape[1:])
    lengths[dim] *= pieces.shape[0]
    return jnp.moveaxis(pieces, 0, dim).reshape(lengths)


def from_everyone(x, axis):
    copies = jnp.broadcast_to(x, (lax.axis_size(axis), *x.shape))
    return lax.all_to_all(copies, axis, split_axis=0, concat_axis=0, tiled=True)


def gathered_copies(x, axis, dim):
    return joined_along(from_everyone(x, axis), dim)


def rotate(values, positions):
    halfway = values.shape[-1] // 2
    inverse = ROTARY_BASE ** (-jnp.arange(halfway, dtype=jnp.float32) / halfway)
    angles = positions.astype(jnp.float32)[:, None, None] * inverse
    cosines, sines = (jnp.cos(angles), jnp.sin(angles))
    leading, trailing = (values[..., :halfway], values[..., halfway:])
    return jnp.concatenate(
        [leading * cosines - trailing * sines, leading * sines + trailing * cosines], axis=-1
    )


def retain(query_rows, key_rows, value_rows, head_start):
    token_count = query_rows.shape[0]
    groups = query_rows.shape[1] // RET_DIM
    layout = (token_count // SEQ_LEN, SEQ_LEN, groups, RET_DIM)
    places = jnp.arange(SEQ_LEN, dtype=jnp.int32)
    rot_query = rotate(query_rows.reshape(layout).astype(jnp.float32), places).astype(jnp.bfloat16)
    rot_key = (
        rotate(key_rows.reshape(layout).astype(jnp.float32), places) * RET_DIM ** (-0.5)
    ).astype(jnp.bfloat16)
    head_number = (head_start + jnp.arange(groups, dtype=jnp.int32)).astype(jnp.float32)
    log_gamma = jnp.log1p(-jnp.exp2(-5.0 - head_number))
    offsets = (places[:, None] - places[None, :]).astype(jnp.float32)
    decays = jnp.where(
        offsets[None] >= 0.0,
        jnp.exp(log_gamma[:, None, None] * jnp.maximum(offsets, 0.0)[None]),
        0.0,
    )
    scores = jnp.einsum("sigd,sjgd->sgij", rot_query, rot_key, preferred_element_type=jnp.float32)
    weights = (scores * decays[None]).astype(jnp.bfloat16)
    output = jnp.einsum(
        "sgij,sjge->sige", weights, value_rows.reshape(layout), preferred_element_type=jnp.float32
    )
    centred = output - jnp.mean(output, -1, keepdims=True)
    normed = centred * lax.rsqrt(jnp.mean(centred * centred, -1, keepdims=True) + NORM_EPS)
    return normed.astype(jnp.bfloat16).reshape(token_count, groups, RET_DIM)


def partial_attend(query_block, kv_rows, head_width):
    leading = kv_rows.shape[:-2]
    groups = query_block.shape[-2]
    split_shape = leading + (kv_rows.shape[-2], groups, HEAD_DIM)
    key_part = kv_rows[..., :head_width].reshape(split_shape)
    value_part = kv_rows[..., head_width:].reshape(split_shape)
    scores = jnp.einsum(
        "...tgd,...rgd->...gtr", query_block, key_part, preferred_element_type=jnp.float32
    ) * HEAD_DIM ** (-0.5)
    highest = jnp.max(scores, -1)
    exponent = jnp.exp(scores - highest[..., None])
    totals = jnp.sum(exponent, -1)
    weighted = jnp.einsum(
        "...gtr,...rgd->...tgd",
        exponent.astype(jnp.bfloat16),
        value_part,
        preferred_element_type=jnp.float32,
    )
    return (
        weighted.astype(jnp.bfloat16).reshape(leading + (query_block.shape[-3], head_width)),
        highest,
        totals,
    )


def combine(weighted, highest, totals, gate_vals):
    block_count, per_block, span_len, head_width = weighted.shape
    groups = highest.shape[2]
    overall = jnp.max(highest, 1, keepdims=True)
    scales = jnp.exp(highest - overall)
    denominator = jnp.sum(scales * totals, 1)
    pieces = (
        lax.optimization_barrier(weighted)
        .reshape(block_count, per_block, span_len, groups, head_width // groups)
        .astype(jnp.float32)
    )
    numerator = jnp.sum(jnp.transpose(scales, (0, 1, 3, 2))[..., None] * pieces, 1)
    gate_cols = gate_vals.reshape(block_count, span_len, groups)[..., None]
    result = gate_cols * numerator / jnp.transpose(denominator, (0, 2, 1))[..., None]
    return result.astype(jnp.bfloat16).reshape(block_count * span_len, groups, head_width // groups)


def body(
    tokens, ret_query, ret_key, ret_value, w_query, w_key, w_value, w_gate, store, passage_ids
):
    owners = lax.axis_size("st")
    head_rank = lax.axis_index("tp")
    groups = w_query.shape[1] // HEAD_DIM
    head_width = groups * HEAD_DIM
    token_count = tokens.shape[0]
    block_count = token_count // BLOCK
    retained = retain(ret_query, ret_key, ret_value, head_rank * groups)
    shard_cols = gathered_copies(tokens, "tp", 1)
    query_sum = jnp.dot(shard_cols, w_query, preferred_element_type=jnp.float32)
    gate_sum = jnp.dot(shard_cols, w_gate, preferred_element_type=jnp.float32)
    gate_vals = jax.nn.sigmoid(lax.dynamic_slice_in_dim(gate_sum, head_rank * groups, groups, 1))
    query_blocks = query_sum.astype(jnp.bfloat16).reshape(block_count, BLOCK, groups, HEAD_DIM)
    kv_own = jnp.concatenate(
        [
            jnp.dot(store, w_key, preferred_element_type=jnp.float32).astype(jnp.bfloat16),
            jnp.dot(store, w_value, preferred_element_type=jnp.float32).astype(jnp.bfloat16),
        ],
        axis=-1,
    )
    flat_ids = passage_ids.reshape(-1)
    requests = flat_ids.shape[0]
    capacity = max(2, 2 * requests // owners)
    owner_of = flat_ids // store.shape[0]
    within = flat_ids % store.shape[0]
    hit_table = (owner_of[:, None] == jnp.arange(owners, dtype=jnp.int32)[None, :]).astype(
        jnp.int32
    )
    earlier = (
        jnp.arange(requests, dtype=jnp.int32)[:, None]
        > jnp.arange(requests, dtype=jnp.int32)[None, :]
    ).astype(jnp.int32)
    slot_of = jnp.sum(jnp.dot(earlier, hit_table) * hit_table, 1)
    placed = (
        hit_table[:, :, None]
        * (slot_of[:, None] == jnp.arange(capacity, dtype=jnp.int32)[None, :]).astype(jnp.int32)[
            :, None, :
        ]
    )
    wanted = jnp.sum(placed * within[:, None, None], 0)
    fetch_at = owner_of * capacity + slot_of
    block_of = jnp.sum(placed * (jnp.arange(requests, dtype=jnp.int32) // NPB)[:, None, None], 0)
    outgoing = jnp.take(query_blocks, block_of, axis=0)
    incoming = lax.all_to_all(outgoing, "st", split_axis=0, concat_axis=0, tiled=True)
    indices = lax.all_to_all(wanted, "st", split_axis=0, concat_axis=0, tiled=True)
    weighted_here, highest_here, totals_here = partial_attend(
        incoming, jnp.take(kv_own, indices, axis=0), head_width
    )
    back_values = lax.all_to_all(weighted_here, "st", split_axis=0, concat_axis=0, tiled=True)
    returned = (
        back_values,
        lax.all_to_all(highest_here, "st", split_axis=0, concat_axis=0, tiled=True),
        lax.all_to_all(totals_here, "st", split_axis=0, concat_axis=0, tiled=True),
    )
    weighted = jnp.take(
        returned[0].reshape((owners * capacity,) + returned[0].shape[2:]), fetch_at, axis=0
    )
    weighted = weighted.reshape(block_count, NPB, BLOCK, head_width)
    highest = jnp.take(
        returned[1].reshape((owners * capacity,) + returned[1].shape[2:]), fetch_at, axis=0
    )
    highest = highest.reshape(block_count, NPB, groups, BLOCK)
    totals = jnp.take(
        returned[2].reshape((owners * capacity,) + returned[2].shape[2:]), fetch_at, axis=0
    )
    totals = totals.reshape(block_count, NPB, groups, BLOCK)
    retrieved = combine(weighted, highest, totals, gate_vals)
    return jnp.concatenate([retained, retrieved], -1).reshape(
        token_count, groups * (RET_DIM + HEAD_DIM)
    )


def solution(mesh):
    placed = (
        P(("grp", "st"), "tp"),
        P(("grp", "st"), "tp"),
        P(("grp", "st"), "tp"),
        P(("grp", "st"), "tp"),
        P(None, "tp"),
        P(None, "tp"),
        P(None, "tp"),
        P(),
        P("st", None, None),
        P(("grp", "st"), None),
    )
    return jax.shard_map(
        body, mesh=mesh, in_specs=placed, out_specs=P(("grp", "st"), "tp"), check_vma=False
    )
```

profile of v0, /device:TPU:40, one launch (start us, length us, event | category | flops | bytes accessed | tf_op | source)
XLA Modules:
  0.0 513.3 jit_solution(3443096300034272680)
XLA Ops:
  0.0 2.2 copy.40
  2.2 2.6 broadcast_in_dim.31
  4.8 4.7 all-to-all-start
  11.2 25.0 %all-to-all-done = bf16[4,512,512]{1,2,0:T(8,128)(2,1)} async-done(((bf16[4,512,512]{1,2,0:T(8,128)(2,1)}), bf16[4,512,512]{1,2,0:T(8,128)(2,1)}, u32[]{:S(2)}, u32[]{:S(2)}) %all-to-all-start) | async-done | bytes 2097184 | tf_op jit(solution)/shard_map/all_to_all | solution.py:25
  36.2 24.7 %all-to-all-start.2 = ((s32[32,1,2]{2,1,0:T(1,128)}), s32[32,1,2]{2,1,0:T(1,128)S(1)}, u32[]{:S(2)}, u32[]{:S(2)}) async-start(s32[32,1,2]{2,1,0:T(1,128)} %copy.47), calls=%async_computation.2 | async-start | bytes 32768 | tf_op jit(solution)/shard_map/all_to_all | solution.py:158
  60.9 4.3 convolution_convert_fusion
  65.2 3.8 gather_fusion
  69.0 4.7 broadcast_select_fusion.1
  73.7 12.4 %all-to-all-start.1 = ((bf16[32,2,64,1,512]{4,2,1,3,0:T(8,128)(2,1)}), bf16[32,2,64,1,512]{4,2,1,3,0:T(8,128)(2,1)}, u32[]{:S(2)}, u32[]{:S(2)}) async-start(bf16[32,2,64,1,512]{4,2,1,3,0:T(8,128)(2,1)} %broadcast_select_fusion.1), calls=%async_computation.1 | async-start | bytes 8388608 | tf_op jit(solution)/shard_map/all_to_all | solution.py:157
  86.1 3.5 fusion.13
  89.6 1.8 fusion.16
  92.1 7.5 %gather_fusion.1 = bf16[64,128,1024]{2,1,0:T(8,128)(2,1)} fusion(bf16[6,128,1024]{2,1,0:T(8,128)(2,1)S(1)} %pad_maximum_fusion, s32[1024]{0:T(1024)S(1)} %pad_clamp_fusion.2), kind=kCustom, calls=%fused_computation.3 | custom fusion | bytes 33554688 | tf_op jit(solution)/shard_map/jit(_take)/gather | solution.py:160
  99.5 14.2 %broadcast_select_fusion = bf16[32,2,128,1024]{3,2,1,0:T(8,128)(2,1)} fusion(bf16[32,2,128,1024]{3,2,1,0:T(8,128)(2,1)} %bitcast.105, pred[32,2]{1,0:T(8,128)(4,1)S(1)} %copy.49), kind=kLoop, calls=%fused_computation.5 | loop fusion | flops 8388608 | bytes 33554496 | tf_op jit(solution)/shard_map/jit(_take)/select_n | solution.py:160
  113.7 155.8 %all-to-all-done.1 = bf16[32,2,64,1,512]{4,2,1,3,0:T(8,128)(2,1)} async-done(((bf16[32,2,64,1,512]{4,2,1,3,0:T(8,128)(2,1)}), bf16[32,2,64,1,512]{4,2,1,3,0:T(8,128)(2,1)}, u32[]{:S(2)}, u32[]{:S(2)}) %all-to-all-start.1) | async-done | bytes 4194336 | tf_op jit(solution)/shard_map/all_to_all | solution.py:157
  269.6 7.7 %multiply_reduce_fusion.1 = (f32[32,2,64]{2,1,0:T(2,128)S(1)}, f32[32,2,64,128]{3,2,1,0:T(8,128)S(1)}) fusion(bf16[32,2,128,1024]{3,2,1,0:T(8,128)(2,1)} %broadcast_select_fusion, bf16[32,2,64,1,512]{4,2,1,3,0:T(8,128)(2,1)} %all-to-all-done.1), kind=kOutput, calls=%fused_computation.20 | convolution fusion | flops 537915392 | bytes 14696448 | tf_op jit(solution)/shard_map/...tgd,...rgd->...gtr/dot_general | solution.py:76
  279.4 10.4 %all-to-all-start.5 = ((f32[32,1,128]{2,1,0:T(1,128)}), f32[32,1,128]{2,1,0:T(1,128)S(1)}, u32[]{:S(2)}, u32[]{:S(2)}) async-start(f32[32,1,128]{2,1,0:T(1,128)} %reshape.719), calls=%async_computation.5 | async-start | bytes 32768 | tf_op jit(solution)/shard_map/all_to_all | solution.py:166
  290.4 11.0 %all-to-all-done.5 = f32[32,1,128]{2,1,0:T(1,128)S(1)} async-done(((f32[32,1,128]{2,1,0:T(1,128)}), f32[32,1,128]{2,1,0:T(1,128)S(1)}, u32[]{:S(2)}, u32[]{:S(2)}) %all-to-all-start.5) | async-done | bytes 16416 | tf_op jit(solution)/shard_map/all_to_all | solution.py:166
  301.5 4.9 all-to-all-start.3
  306.4 5.6 %convert_bitcast_fusion = bf16[32,2,64,512]{3,2,1,0:T(8,128)(2,1)} fusion(bf16[32,2,128,1024]{3,2,1,0:T(8,128)(2,1)} %broadcast_select_fusion, f32[32,2,64,128]{3,2,1,0:T(8,128)S(1)} %get-tuple-element.27, f32[32,2,64]{2,1,0:T(2,128)S(1)} %get-tuple-element.26), kind=kOutput, calls=%fused_computation.12 | convolution fusion | flops 540540928 | bytes 14696448 | tf_op jit(solution)/shard_map/...gtr,...rgd->...tgd/dot_general | solution.py:82
  311.9 6.2 %all-to-all-done.3 = f32[32,1,128]{2,1,0:T(1,128)S(1)} async-done(((f32[32,1,128]{2,1,0:T(1,128)}), f32[32,1,128]{2,1,0:T(1,128)S(1)}, u32[]{:S(2)}, u32[]{:S(2)}) %all-to-all-start.3) | async-done | bytes 16416 | tf_op jit(solution)/shard_map/all_to_all | solution.py:165
  318.1 6.4 %all-to-all-start.4 = ((bf16[32,2,64,512]{3,2,1,0:T(8,128)(2,1)}), bf16[32,2,64,512]{3,2,1,0:T(8,128)(2,1)}, u32[]{:S(2)}, u32[]{:S(2)}) async-start(bf16[32,2,64,512]{3,2,1,0:T(8,128)(2,1)} %convert_bitcast_fusion), calls=%async_computation.4 | async-start | bytes 8388608 | tf_op jit(solution)/shard_map/all_to_all | solution.py:162
  326.9 2.0 fusion.61
  332.3 175.7 %all-to-all-done.4 = bf16[32,2,64,512]{3,2,1,0:T(8,128)(2,1)} async-done(((bf16[32,2,64,512]{3,2,1,0:T(8,128)(2,1)}), bf16[32,2,64,512]{3,2,1,0:T(8,128)(2,1)}, u32[]{:S(2)}, u32[]{:S(2)}) %all-to-all-start.4) | async-done | bytes 4194336 | tf_op jit(solution)/shard_map/all_to_all | solution.py:162
  508.0 2.9 gather_fusion.2
  (86 shorter events, 13.1 us)
Async XLA Ops:
  0.0 86.1 %copy-start = (bf16[6,128,2048]{2,1,0:T(8,128)(2,1)S(1)}, bf16[6,128,2048]{2,1,0:T(8,128)(2,1)}, u32[]{:S(2)}) copy-start(bf16[6,128,2048]{2,1,0:T(8,128)(2,1)} %param.20) | copy-start | bytes 9437188
  4.8 4.7 copy-start.6
  4.8 31.4 %all-to-all-start = ((bf16[4,512,512]{1,2,0:T(8,128)(2,1)}), bf16[4,512,512]{1,2,0:T(8,128)(2,1)}, u32[]{:S(2)}, u32[]{:S(2)}) async-start(bf16[4,512,512]{1,2,0:T(8,128)(2,1)} %broadcast_in_dim.31), calls=%async_computation | async-start | bytes 4194304 | tf_op jit(solution)/shard_map/all_to_all | solution.py:25
  36.2 37.5 %all-to-all-start.2 = ((s32[32,1,2]{2,1,0:T(1,128)}), s32[32,1,2]{2,1,0:T(1,128)S(1)}, u32[]{:S(2)}, u32[]{:S(2)}) async-start(s32[32,1,2]{2,1,0:T(1,128)} %copy.47), calls=%async_computation.2 | async-start | bytes 32768 | tf_op jit(solution)/shard_map/all_to_all | solution.py:158
  73.7 195.9 %all-to-all-start.1 = ((bf16[32,2,64,1,512]{4,2,1,3,0:T(8,128)(2,1)}), bf16[32,2,64,1,512]{4,2,1,3,0:T(8,128)(2,1)}, u32[]{:S(2)}, u32[]{:S(2)}) async-start(bf16[32,2,64,1,512]{4,2,1,3,0:T(8,128)(2,1)} %broadcast_select_fusion.1), calls=%async_computation.1 | async-start | bytes 8388608 | tf_op jit(solution)/shard_map/all_to_all | solution.py:157
  86.1 3.5 copy-start.7
  279.4 22.1 %all-to-all-start.5 = ((f32[32,1,128]{2,1,0:T(1,128)}), f32[32,1,128]{2,1,0:T(1,128)S(1)}, u32[]{:S(2)}, u32[]{:S(2)}) async-start(f32[32,1,128]{2,1,0:T(1,128)} %reshape.719), calls=%async_computation.5 | async-start | bytes 32768 | tf_op jit(solution)/shard_map/all_to_all | solution.py:166
  301.5 16.6 %all-to-all-start.3 = ((f32[32,1,128]{2,1,0:T(1,128)}), f32[32,1,128]{2,1,0:T(1,128)S(1)}, u32[]{:S(2)}, u32[]{:S(2)}) async-start(f32[32,1,128]{2,1,0:T(1,128)} %reshape.717), calls=%async_computation.3 | async-start | bytes 32768 | tf_op jit(solution)/shard_map/all_to_all | solution.py:165
  311.9 12.8 %copy-start.2 = (bf16[512,256]{1,0:T(8,128)(2,1)S(1)}, bf16[512,256]{1,0:T(8,128)(2,1)}, u32[]{:S(2)}) copy-start(bf16[512,256]{1,0:T(8,128)(2,1)} %param.13) | copy-start | bytes 786436
  311.9 12.9 %copy-start.3 = (bf16[512,256]{1,0:T(8,128)(2,1)S(1)}, bf16[512,256]{1,0:T(8,128)(2,1)}, u32[]{:S(2)}) copy-start(bf16[512,256]{1,0:T(8,128)(2,1)} %param.14) | copy-start | bytes 786436
  318.1 189.9 %all-to-all-start.4 = ((bf16[32,2,64,512]{3,2,1,0:T(8,128)(2,1)}), bf16[32,2,64,512]{3,2,1,0:T(8,128)(2,1)}, u32[]{:S(2)}, u32[]{:S(2)}) async-start(bf16[32,2,64,512]{3,2,1,0:T(8,128)(2,1)} %convert_bitcast_fusion), calls=%async_computation.4 | async-start | bytes 8388608 | tf_op jit(solution)/shard_map/all_to_all | solution.py:162
  324.8 1.1 copy-start.4
  325.8 1.0 copy-start.5
  511.1 2.2 copy-start.1
where the time goes:
time: 518 us; the launch traced here: 513 us
  waiting for transfers between devices  374 us (72%)
  starting transfers between devices  63.5 us (12%)
  matrix products  25.5 us (5%)
  other arithmetic  25.4 us (5%)
  local copies, waits for them, and re-layouts  24.8 us (5%)
    all_to_all x1, waiting for transfers between devices, body(): lax.all_to_all(weighted_here, 'st', split_axis=0, concat_axis=0, tiled=True)  176 us
    all_to_all x1, waiting for transfers between devices, body(): lax.all_to_all(outgoing, 'st', split_axis=0, concat_axis=0, tiled=True)  156 us
    all_to_all x1, waiting for transfers between devices, from_everyone(): return lax.all_to_all(copies, axis, split_axis=0, concat_axis=0, tiled=True)  25 us
    all_to_all x1, starting transfers between devices, body(): lax.all_to_all(wanted, 'st', split_axis=0, concat_axis=0, tiled=True)  24.7 us
    select_n x2, other arithmetic, body(): jnp.take(kv_own, indices, axis=0)  14.2 us
    all_to_all x1, starting transfers between devices, body(): lax.all_to_all(outgoing, 'st', split_axis=0, concat_axis=0, tiled=True)  12.4 us
    all_to_all x1, waiting for transfers between devices, body(): lax.all_to_all(totals_here, 'st', split_axis=0, concat_axis=0, tiled=True)  11 us
    all_to_all x1, starting transfers between devices, body(): lax.all_to_all(totals_here, 'st', split_axis=0, concat_axis=0, tiled=True)  10.4 us
  transfers between devices with their start and end apart: 6, of which 5 were waited for; matrix products, arithmetic and copies ran while one was open for 11% of the time, Pallas kernels for 0%

commit v1 on v0

v1 whole, which is shorter than its diff:
```python
import functools

import jax
import jax.numpy as jnp
from jax import lax
from jax.experimental import pallas as pl
from jax.experimental.pallas import tpu as pltpu
from jax.sharding import PartitionSpec as P

RET_DIM = 256
HEAD_DIM = 512
BLOCK = 64
NPB = 4
SEQ_LEN = 256
CAP = 2
CORES = 2
CHUNK = 128
ROTARY_BASE = 10000.0
NORM_EPS = 1e-05
MASKED = -1e30
FLOOR = -1e28


def rotate(values, positions):
    halfway = values.shape[-1] // 2
    inverse = ROTARY_BASE ** (-jnp.arange(halfway, dtype=jnp.float32) / halfway)
    angles = positions.astype(jnp.float32)[:, None, None] * inverse
    cosines, sines = (jnp.cos(angles), jnp.sin(angles))
    leading, trailing = (values[..., :halfway], values[..., halfway:])
    return jnp.concatenate(
        [leading * cosines - trailing * sines, leading * sines + trailing * cosines], axis=-1
    )


def retain(query_rows, key_rows, value_rows, head_start):
    token_count = query_rows.shape[0]
    groups = query_rows.shape[1] // RET_DIM
    layout = (token_count // SEQ_LEN, SEQ_LEN, groups, RET_DIM)
    places = jnp.arange(SEQ_LEN, dtype=jnp.int32)
    rot_query = rotate(query_rows.reshape(layout).astype(jnp.float32), places).astype(jnp.bfloat16)
    rot_key = (
        rotate(key_rows.reshape(layout).astype(jnp.float32), places) * RET_DIM ** (-0.5)
    ).astype(jnp.bfloat16)
    head_number = (head_start + jnp.arange(groups, dtype=jnp.int32)).astype(jnp.float32)
    log_gamma = jnp.log1p(-jnp.exp2(-5.0 - head_number))
    offsets = (places[:, None] - places[None, :]).astype(jnp.float32)
    decays = jnp.where(
        offsets[None] >= 0.0,
        jnp.exp(log_gamma[:, None, None] * jnp.maximum(offsets, 0.0)[None]),
        0.0,
    )
    scores = jnp.einsum("sigd,sjgd->sgij", rot_query, rot_key, preferred_element_type=jnp.float32)
    weights = (scores * decays[None]).astype(jnp.bfloat16)
    output = jnp.einsum(
        "sgij,sjge->sige", weights, value_rows.reshape(layout), preferred_element_type=jnp.float32
    )
    centred = output - jnp.mean(output, -1, keepdims=True)
    normed = centred * lax.rsqrt(jnp.mean(centred * centred, -1, keepdims=True) + NORM_EPS)
    return normed.astype(jnp.bfloat16).reshape(token_count, groups, RET_DIM)


def ring_kernel(
    pid_ref, blk_ref, q_ref, k_ref, v_ref, out_ref, ml_ref,
    qbuf, kall, vall, loc, locml, loc0, loc0ml, rbuf, rml,
    local_sem, kv_send, kv_recv, q_send, q_recv, r_send, r_recv, s_send, s_recv,
):
    devices = lax.axis_size("st")
    ring = devices // CORES
    far = ring // 2
    chunks = q_ref.shape[0]
    half = chunks // 2
    slots = CAP * CORES
    mine = lax.axis_index("st")
    place, core = mine // CORES, mine % CORES
    right = lax.rem(mine + CORES, devices)
    left = lax.rem(mine + devices - CORES, devices)
    partner = mine + 1 - 2 * core
    toward = (right, left)
    far_set = (tuple(range(half)), tuple(range(half, chunks)))

    barrier = pltpu.get_barrier_semaphore()
    for device in (right, left, partner):
        pl.semaphore_signal(barrier, inc=1, device_id={"st": device})
    pl.semaphore_wait(barrier, 3)

    def q_copy(way, hop, j):
        source = q_ref.at[j] if isinstance(hop, int) and hop == 1 else qbuf.at[way, jnp.maximum(hop - 2, 0), j]
        return pltpu.make_async_remote_copy(
            src_ref=source,
            dst_ref=qbuf.at[way, hop - 1, j],
            send_sem=q_send.at[way, hop - 1, j],
            recv_sem=q_recv.at[way, hop - 1, j],
            device_id={"st": toward[way]},
        )

    for j in range(chunks):
        for way in range(2):
            q_copy(way, 1, j).start()

    kv_copies = []
    for i, (own, everyone) in enumerate(((k_ref, kall), (v_ref, vall))):
        kv_copies.append(
            pltpu.make_async_remote_copy(
                src_ref=own,
                dst_ref=everyone.at[core],
                send_sem=kv_send.at[i],
                recv_sem=kv_recv.at[i],
                device_id={"st": partner},
            )
        )
    local_copies = [
        pltpu.make_async_copy(own, everyone.at[core], local_sem.at[i])
        for i, (own, everyone) in enumerate(((k_ref, kall), (v_ref, vall)))
    ]
    for copy in kv_copies:
        copy.start()
    for copy in local_copies:
        copy.start()
    for copy in local_copies:
        copy.wait()
    for copy in kv_copies:
        copy.wait()

    passages = k_ref.shape[0]
    lanes = lax.broadcasted_iota(jnp.int32, (1, CHUNK), 1)

    def attend(query, source, j):
        base = source * slots
        keys, values, penalties = [], [], []
        for slot in range(slots):
            passage = pid_ref[base + slot]
            block = blk_ref[base + slot]
            keys.append(kall[passage // passages, passage % passages])
            values.append(vall[passage // passages, passage % passages])
            within = block - j * (CHUNK // BLOCK)
            penalties.append(jnp.where(lanes // BLOCK == within, 0.0, MASKED))
        scores = [
            jnp.dot(key, query, preferred_element_type=jnp.float32) * HEAD_DIM ** (-0.5) + penalty
            for key, penalty in zip(keys, penalties)
        ]
        highest = jnp.full((1, CHUNK), FLOOR, jnp.float32)
        for score in scores:
            highest = jnp.maximum(highest, jnp.max(score, 0, keepdims=True))
        exponents = [jnp.exp(score - highest) for score in scores]
        total = jnp.zeros((1, CHUNK), jnp.float32)
        for exponent in exponents:
            total = total + jnp.sum(exponent, 0, keepdims=True)
        weighted = jnp.dot(
            jnp.concatenate(values, 1),
            jnp.concatenate([e.astype(jnp.bfloat16) for e in exponents], 0),
            preferred_element_type=jnp.float32,
        )
        return weighted, highest, total

    def source_of(way, hop):
        return lax.rem(place + (ring - hop if way == 0 else hop), ring)

    def attend_hop(hop, ways_chunks):
        for way, j in ways_chunks:
            weighted, highest, total = attend(qbuf[way, hop - 1, j], source_of(way, hop), j)
            loc[way, hop - 1, j] = weighted.astype(jnp.bfloat16)
            locml[way, hop - 1, j, 0:1] = highest
            locml[way, hop - 1, j, 1:2] = total

    @pl.loop(0, chunks)
    def _(j):
        weighted, highest, total = attend(q_ref[j], place, j)
        loc0[j] = weighted.astype(jnp.bfloat16)
        loc0ml[j, 0:1] = highest
        loc0ml[j, 1:2] = total

    def arrive(hop, forward):
        for j in range(chunks):
            for way in range(2):
                q_copy(way, hop, j).wait_recv()
                if j in forward[way]:
                    q_copy(way, hop + 1, j).start()

    everything = (tuple(range(chunks)),) * 2

    @pl.loop(1, far - 1)
    def _(hop):
        arrive(hop, everything)

        @pl.loop(0, chunks)
        def _(j):
            attend_hop(hop, [(0, j), (1, j)])

    arrive(far - 1, far_set)

    @pl.loop(0, chunks)
    def _(j):
        attend_hop(far - 1, [(0, j), (1, j)])

    def r_copies(way, hop, j):
        data = pltpu.make_async_remote_copy(
            src_ref=loc.at[1 - way, hop - 1, j],
            dst_ref=rbuf.at[way, hop - 1, j],
            send_sem=r_send.at[way, hop - 1, j],
            recv_sem=r_recv.at[way, hop - 1, j],
            device_id={"st": toward[way]},
        )
        stats = pltpu.make_async_remote_copy(
            src_ref=locml.at[1 - way, hop - 1, j],
            dst_ref=rml.at[way, hop - 1, j],
            send_sem=s_send.at[way, hop - 1, j],
            recv_sem=s_recv.at[way, hop - 1, j],
            device_id={"st": toward[way]},
        )
        return data, stats

    def r_start(way, hop, j):
        for copy in r_copies(way, hop, j):
            copy.start()

    def merge(first, first_ml, second, second_ml):
        top = jnp.maximum(first_ml[0], second_ml[0])
        left_scale, right_scale = jnp.exp(first_ml[0] - top), jnp.exp(second_ml[0] - top)
        summed = first * left_scale + second * right_scale
        total = first_ml[1] * left_scale + second_ml[1] * right_scale
        return summed, (top, total)

    def r_merge(way, hop, j):
        for copy in r_copies(way, hop + 1, j):
            copy.wait_recv()
        summed, (top, total) = merge(
            rbuf[way, hop, j].astype(jnp.float32),
            (rml[way, hop, j, 0:1], rml[way, hop, j, 1:2]),
            loc[1 - way, hop - 1, j].astype(jnp.float32),
            (locml[1 - way, hop - 1, j, 0:1], locml[1 - way, hop - 1, j, 1:2]),
        )
        loc[1 - way, hop - 1, j] = summed.astype(jnp.bfloat16)
        locml[1 - way, hop - 1, j, 0:1] = top
        locml[1 - way, hop - 1, j, 1:2] = total

    for i in range(half):
        for way in range(2):
            q_copy(way, far, far_set[way][i]).wait_recv()
        attend_hop(far, [(way, far_set[way][i]) for way in range(2)])
    for i in range(half):
        for way in range(2):
            r_start(way, far, far_set[1 - way][i])

    for i in range(half):
        for way in range(2):
            r_start(way, far - 1, far_set[way][i])
    for i in range(half):
        for way in range(2):
            r_merge(way, far - 1, far_set[1 - way][i])
        for way in range(2):
            r_start(way, far - 1, far_set[1 - way][i])

    @pl.loop(1, far - 1)
    def _(step):
        hop = far - 1 - step
        for j in range(chunks):
            order = [(way, (far_set[way] + far_set[1 - way])[j]) for way in range(2)]
            for way, chunk in order:
                r_merge(way, hop, chunk)
            for way, chunk in order:
                r_start(way, hop, chunk)

    for i in range(chunks):
        for way in range(2):
            for copy in r_copies(way, 1, (far_set[way] + far_set[1 - way])[i]):
                copy.wait_recv()

    @pl.loop(0, chunks)
    def _(j):
        summed, both = loc0[j].astype(jnp.float32), (loc0ml[j, 0:1], loc0ml[j, 1:2])
        for way in range(2):
            summed, both = merge(
                summed, both, rbuf[way, 0, j].astype(jnp.float32), (rml[way, 0, j, 0:1], rml[way, 0, j, 1:2])
            )
        out_ref[j] = summed
        ml_ref[j, 0:1] = both[0]
        ml_ref[j, 1:2] = both[1]

    for j in range(chunks):
        for way in range(2):
            q_copy(way, 1, j).wait_send()

    @pl.loop(2, far)
    def _(hop):
        for j in range(chunks):
            for way in range(2):
                q_copy(way, hop, j).wait_send()

    @pl.loop(1, far)
    def _(hop):
        for j in range(chunks):
            for way in range(2):
                for copy in r_copies(way, hop, j):
                    copy.wait_send()

    for way in range(2):
        for j in far_set[way]:
            q_copy(way, far, j).wait_send()
        for j in far_set[1 - way]:
            for copy in r_copies(way, far, j):
                copy.wait_send()


def ring_attend(pids, blocks, queries, keys, values):
    ring = lax.axis_size("st") // CORES
    far = ring // 2
    chunks, width, _ = queries.shape
    passages, rows, _ = keys.shape
    buffer = (2, far, chunks, width, CHUNK)
    stats = (2, far, chunks, 2, CHUNK)
    flags = (2, far, chunks)
    dma = pltpu.SemaphoreType.DMA
    return pl.pallas_call(
        ring_kernel,
        out_shape=(
            jax.ShapeDtypeStruct((chunks, width, CHUNK), jnp.float32),
            jax.ShapeDtypeStruct((chunks, 2, CHUNK), jnp.float32),
        ),
        in_specs=[pl.BlockSpec(memory_space=pltpu.SMEM)] * 2
        + [pl.BlockSpec(memory_space=pltpu.VMEM)] * 3,
        out_specs=(pl.BlockSpec(memory_space=pltpu.VMEM),) * 2,
        scratch_shapes=[
            pltpu.VMEM(buffer, jnp.bfloat16),
            pltpu.VMEM((CORES, passages, rows, width), jnp.bfloat16),
            pltpu.VMEM((CORES, passages, width, rows), jnp.bfloat16),
            pltpu.VMEM(buffer, jnp.bfloat16),
            pltpu.VMEM(stats, jnp.float32),
            pltpu.VMEM(buffer[2:], jnp.bfloat16),
            pltpu.VMEM(stats[2:], jnp.float32),
            pltpu.VMEM(buffer, jnp.bfloat16),
            pltpu.VMEM(stats, jnp.float32),
            dma((2,)),
            dma((2,)),
            dma((2,)),
            dma(flags),
            dma(flags),
            dma(flags),
            dma(flags),
            dma(flags),
            dma(flags),
        ],
        compiler_params=pltpu.CompilerParams(
            collective_id=0, has_side_effects=True, vmem_limit_bytes=60 * 1024 * 1024
        ),
    )(pids, blocks, queries, keys, values)


def slot_tables(passage_ids, per_chip):
    ring = lax.axis_size("st") // CORES
    mine = lax.axis_index("st")
    place, core = mine // CORES, mine % CORES
    ids = lax.all_gather(passage_ids.reshape(1, -1), "st", axis=0, tiled=True)
    ids = ids.reshape(ring, CORES, -1)
    ids = jnp.where(core == 0, ids[:, 0], ids[:, 1])
    hit = (ids // per_chip == place).astype(jnp.int32)
    requests = ids.shape[1]
    order = jnp.arange(requests, dtype=jnp.int32)
    earlier = (order[:, None] > order[None, :]).astype(jnp.int32)
    rank = jnp.sum(hit[:, None, :] * earlier[None], -1)
    slots = jnp.arange(CAP * CORES, dtype=jnp.int32)
    chosen = hit[:, None, :] * (rank[:, None, :] == slots[None, :, None]).astype(jnp.int32)
    pids = jnp.sum(chosen * (ids % per_chip)[:, None, :], -1)
    blocks = jnp.sum(chosen * (order // NPB + 1)[None, None, :], -1) - 1
    blocks = jnp.where(blocks < 0, -CHUNK, blocks)
    return pids.reshape(-1), blocks.reshape(-1)


def body(
    tokens, ret_query, ret_key, ret_value, w_query, w_key, w_value, w_gate, store, passage_ids
):
    head_rank = lax.axis_index("tp")
    groups = w_query.shape[1] // HEAD_DIM
    token_count = tokens.shape[0]
    passages, rows, features = store.shape
    pids, blocks = slot_tables(passage_ids, passages * CORES)
    retained = retain(ret_query, ret_key, ret_value, head_rank * groups)
    whole = lax.all_gather(tokens, "tp", axis=1, tiled=True)
    queries = jnp.dot(whole, w_query, preferred_element_type=jnp.float32).astype(jnp.bfloat16)
    queries = queries.reshape(token_count // CHUNK, CHUNK, HEAD_DIM).transpose(0, 2, 1)
    gate_sum = jnp.dot(whole, w_gate, preferred_element_type=jnp.float32)
    gate_vals = jax.nn.sigmoid(lax.dynamic_slice_in_dim(gate_sum, head_rank * groups, groups, 1))
    keys = jnp.dot(store, w_key, preferred_element_type=jnp.float32).astype(jnp.bfloat16)
    values = jnp.dot(store, w_value, preferred_element_type=jnp.float32).astype(jnp.bfloat16)
    summed, stats = ring_attend(pids, blocks, queries, keys, values.transpose(0, 2, 1))
    gate_rows = gate_vals.reshape(token_count // CHUNK, 1, CHUNK)
    result = gate_rows * summed / stats[:, 1:2]
    retrieved = result.astype(jnp.bfloat16).transpose(0, 2, 1).reshape(token_count, groups, HEAD_DIM)
    return jnp.concatenate([retained, retrieved], -1).reshape(
        token_count, groups * (RET_DIM + HEAD_DIM)
    )


def solution(mesh):
    placed = (
        P(("grp", "st"), "tp"),
        P(("grp", "st"), "tp"),
        P(("grp", "st"), "tp"),
        P(("grp", "st"), "tp"),
        P(None, "tp"),
        P(None, "tp"),
        P(None, "tp"),
        P(),
        P("st", None, None),
        P(("grp", "st"), None),
    )
    return jax.shard_map(
        body, mesh=mesh, in_specs=placed, out_specs=P(("grp", "st"), "tp"), check_vma=False
    )
```

time: 518 us -> 283 us (0.55)
  waiting for transfers between devices: 374 us -> 0.75 us
  Pallas kernels: 0 us -> 183 us
  starting transfers between devices: 63.5 us -> 0.01 us
  blocking collectives: 0 us -> 49.2 us
  local copies, waits for them, and re-layouts: 24.8 us -> 6.78 us
  between operations: 0.5 us -> 13.7 us
  other arithmetic: 25.4 us -> 13 us
  matrix products: 25.5 us -> 16 us
    all_to_all x6 -> x0, waiting for transfers between devices: 374 us -> none  [the longest x1 176 us: body(): lax.all_to_all(weighted_here, 'st', split_axis=0, concat_axis=0, tiled=True)]
    pallas_call x0 -> x1, Pallas kernels: none -> 183 us  [ring_attend(): pl.pallas_call(ring_kernel, out_shape=(jax.ShapeDtypeStruct((chunks, widt...]
    all_to_all x6 -> x0, starting transfers between devices: 63.5 us -> none  [the longest x1 24.7 us: body(): lax.all_to_all(wanted, 'st', split_axis=0, concat_axis=0, tiled=True)]
    all_gather x0 -> x1, blocking collectives: none -> 49.2 us  [slot_tables(): ids = lax.all_gather(passage_ids.reshape(1, -1), 'st', axis=0, tiled=True)]
    select_n x8 -> x2, other arithmetic: 19.3 us -> 0.6 us  [the longest x1 0.55 us: slot_tables(): blocks = jnp.where(blocks < 0, -CHUNK, blocks)]
    gather x5 -> x0, local copies, waits for them, and re-layouts: 15.2 us -> none  [the longest x1 7.45 us: body(): jnp.take(kv_own, indices, axis=0)]
    dot_general x5 -> x2, matrix products: 19.7 us -> 6.5 us  [the longest x1 4.27 us: body(): jnp.dot(whole, w_query, preferred_element_type=jnp.float32)]
  transfers between devices with their start and end apart: 6 -> 1, of which waited for: 5 -> 0; matrix products, arithmetic and copies ran while one was open for 11% -> 8% of each run, Pallas kernels for 0% -> 0%
where the time goes in v1:
time: 283 us
  Pallas kernels  183 us (65%)
  blocking collectives  49.2 us (17%)
  matrix products  16 us (6%)
  between operations  13.7 us (5%)
  other arithmetic  13 us (5%)
  local copies, waits for them, and re-layouts  6.78 us (2%)
    pallas_call x1, Pallas kernels, ring_attend(): pl.pallas_call(ring_kernel, out_shape=(jax.ShapeDtypeStruct((chunks, widt...  183 us
    all_gather x1, blocking collectives, slot_tables(): ids = lax.all_gather(passage_ids.reshape(1, -1), 'st', axis=0, tiled=True)  49.2 us
  transfers between devices with their start and end apart: 1, of which 0 were waited for; matrix products, arithmetic and copies ran while one was open for 8% of the time, Pallas kernels for 0%

profile of v1, /device:TPU:40, one launch (start us, length us, event | category | flops | bytes accessed | tf_op | source)
XLA Modules:
  0.0 282.5 jit_solution(7005189207764350367)
XLA Ops:
  6.6 0.7 all-gather.3.cloned.1.call-update
  7.4 0.9 copy.21
  8.3 49.2 %all-gather = s32[32,1,32]{2,1,0:T(1,128)S(1)} all-gather(s32[1,1,32]{2,1,0:T(1,128)S(1)} %reshape.276), channel_id=1, replica_groups=mesh['grp'=2,'st'=32,'tp'=4] {'st'}, dimensions={0}, use_global_device_ids=true | all-gather | bytes 4224 | tf_op jit(solution)/shard_map/all_gather | solution.py:352
  57.6 0.4 multiply_reduce_fusion.1
  58.0 0.2 fusion.30
  58.6 0.7 reshape.266.pid_ref
  59.2 1.8 convert.13
  61.0 1.8 convert.14
  62.9 0.5 multiply_cosine_fusion
  63.4 2.1 fusion.27
  65.5 2.4 fusion.39
  67.9 1.3 multiply_reduce_fusion
  69.2 0.6 compare_select_fusion.blk_ref
  69.7 1.2 multiply_convert_fusion
  71.0 4.4 %fusion.4.k_ref = bf16[6,128,512]{2,1,0:T(8,128)(2,1)} fusion(bf16[6,128,2048]{2,1,0:T(8,128)(2,1)S(1)} %copy-done, bf16[2048,512]{1,0:T(8,128)(2,1)} %param.15), kind=kOutput, calls=%fused_computation.4 | convolution fusion | flops 1611005952 | bytes 6029312 | tf_op jit(solution)/shard_map/dot_general | solution.py:382
  75.4 2.7 fusion.10.v_ref
  78.1 4.3 %convolution_convert_fusion = bf16[512,512]{1,0:T(8,128)(2,1)} fusion(bf16[512,2048]{1,0:T(8,128)(2,1)} %all-gather.3.cloned.1.call-done, bf16[2048,512]{1,0:T(8,128)(2,1)} %param.14), kind=kOutput, calls=%fused_computation.6 | convolution fusion | flops 1074003968 | bytes 4718592 | tf_op jit(solution)/shard_map/dot_general | solution.py:378
  82.4 2.1 copy.24
  84.5 183.2 %shard_map.100 = (f32[4,512,128]{2,1,0:T(8,128)}, f32[4,2,128]{2,1,0:T(2,128)}) custom-call(s32[64]{0:T(128)} %reshape.266.pid_ref, s32[64]{0:T(128)} %compare_select_fusion.blk_ref, bf16[4,512,128]{2,1,0:T(8,128)(2,1)} %bitcast.54, bf16[6,128,512]{2,1,0:T(8,128)(2,1)} %fusion.4.k_ref, bf16[6,512,128]{2,1,0:T(8,128)(2,1)} %fusion.10.v_ref), custom_call_target="tpu_custom_call" | custom-call | tf_op jit(solution)/shard_map/pallas_call | solution.py:313
  267.7 0.8 slice.27
  268.5 2.2 fusion.44
  270.8 0.9 fusion.15
  271.7 2.0 copy.26
  273.7 2.0 maximum_bitcast_fusion
  (25 shorter events, 0.6 us)
Async XLA Ops:
  6.5 64.4 %copy-start = (bf16[6,128,2048]{2,1,0:T(8,128)(2,1)S(1)}, bf16[6,128,2048]{2,1,0:T(8,128)(2,1)}, u32[]{:S(2)}) copy-start(bf16[6,128,2048]{2,1,0:T(8,128)(2,1)} %param.18) | copy-start | bytes 9437188
  6.6 71.6 %all-gather.3.cloned.1.call-start = ((), (), s32[]{:S(2)}) async-start(), calls=%async_computation | async-start | bytes 2621440 | tf_op jit(solution)/shard_map/all_gather | solution.py:377
  71.0 4.4 %copy-start.3 = (bf16[2048,512]{1,0:T(8,128)(2,1)S(1)}, bf16[2048,512]{1,0:T(8,128)(2,1)}, u32[]{:S(2)}) copy-start(bf16[2048,512]{1,0:T(8,128)(2,1)} %param.16) | copy-start | bytes 6291460
  82.4 186.1 %copy-start.2 = (bf16[2048,4]{0,1:T(4,128)(2,1)S(1)}, bf16[2048,4]{0,1:T(4,128)(2,1)}, u32[]{:S(2)}) copy-start(bf16[2048,4]{0,1:T(4,128)(2,1)} %param.17) | copy-start | bytes 49156
  267.7 3.0 %copy-start.1 = (f32[4,512,128]{2,1,0:T(8,128)S(1)}, f32[4,512,128]{2,1,0:T(8,128)}, u32[]{:S(2)}) copy-start(f32[4,512,128]{2,1,0:T(8,128)} %get-tuple-element.7) | copy-start | bytes 3145732
Sparse Core Ops, SparseCore 0:
  9.2 50.0 all-gather.2

commit v2 on v1

v2 whole, which is shorter than its diff:
```python
import math

import jax
import jax.numpy as jnp
import numpy as np
from jax import lax
from jax.experimental import pallas as pl
from jax.experimental.pallas import tpu as pltpu
from jax.sharding import PartitionSpec as P

RET_DIM = 256
HEAD_DIM = 512
BLOCK = 64
NPB = 4
SEQ_LEN = 256
CAP = 2
CORES = 2
CHUNK = 128
ROTARY_BASE = 10000.0
NORM_EPS = 1e-05
MASKED = -1e30
FLOOR = -1e28
KV_PARTS = 2


def rotary_tables():
    halfway = RET_DIM // 2
    inverse = np.float32(ROTARY_BASE) ** (-np.arange(halfway, dtype=np.float32) / np.float32(halfway))
    angles = np.arange(SEQ_LEN, dtype=np.float32)[:, None] * inverse.astype(np.float32)
    return np.cos(angles).astype(np.float32), np.sin(angles).astype(np.float32)


def mixer_kernel(
    ids_ref, tokens_hbm, rq_hbm, rk_hbm, rv_hbm, wq_hbm, wk_hbm, wv_hbm, wg_hbm, store_hbm, cos_hbm, sin_hbm,
    out_ref,
    tbuf, wq, wk, wv, wg, store, rq, rk, rv, cosines, sines,
    ids_s, pid_s, blk_s, ids_in, qown, gate, qbuf, kall, vall, loc, locml, loc0, loc0ml, rbuf, rml,
    in_sem, ids_sem, t_sem, kv_send, kv_recv, x_send, x_recv, m_send, m_recv, q_send, q_recv,
    r_send, r_recv, s_send, s_recv,
):
    devices = lax.axis_size("st")
    ring = devices // CORES
    far = ring // 2
    chunks = qown.shape[0]
    half = chunks // 2
    slots = CAP * CORES
    mine = lax.axis_index("st")
    place, core = mine // CORES, mine % CORES
    right = lax.rem(mine + CORES, devices)
    left = lax.rem(mine + devices - CORES, devices)
    partner = mine + 1 - 2 * core
    toward = (right, left)
    xs = lax.axis_size("tp")
    head = lax.axis_index("tp")
    x_right, x_left = lax.rem(head + 1, xs), lax.rem(head + xs - 1, xs)
    x_toward = (x_right, x_left)
    x_source = (head, x_left, x_right, lax.rem(head + 2, xs))
    far_set = (tuple(range(0, chunks, 2)), tuple(range(1, chunks, 2)))
    send_order = (far_set[0] + far_set[1], far_set[1] + far_set[0])
    passages = kall.shape[1]
    rows = kall.shape[2]
    width = tokens_hbm.shape[1]
    ways = range(2)

    loads = [
        pltpu.make_async_copy(source, target, in_sem.at[i])
        for i, (source, target) in enumerate(
            (
                (store_hbm, store), (wk_hbm, wk), (wv_hbm, wv), (wq_hbm, wq), (wg_hbm, wg),
                (rq_hbm, rq), (rk_hbm, rk), (rv_hbm, rv), (cos_hbm, cosines), (sin_hbm, sines),
            )
        )
    ]
    token_loads = [
        pltpu.make_async_copy(tokens_hbm.at[pl.ds(j * CHUNK, CHUNK)], tbuf.at[j, 0], t_sem.at[j])
        for j in range(chunks)
    ]
    for copy in loads[:5]:
        copy.start()
    for copy in token_loads:
        copy.start()

    barrier = pltpu.get_barrier_semaphore()
    for device in (right, left, partner):
        pl.semaphore_signal(barrier, inc=1, device_id={"st": device})
    for device in x_toward:
        pl.semaphore_signal(barrier, inc=1, device_id={"tp": device})
    pl.semaphore_wait(barrier, 5)

    def x_copy(way, hop, j):
        if hop == 1:
            source, target = tokens_hbm.at[pl.ds(j * CHUNK, CHUNK)], tbuf.at[j, 1 + way]
        else:
            part = pl.ds(way * (CHUNK // 2), CHUNK // 2)
            source, target = tbuf.at[j, 1 + way, part], tbuf.at[j, 3, part]
        return pltpu.make_async_remote_copy(
            src_ref=source,
            dst_ref=target,
            send_sem=x_send.at[way, hop - 1, j],
            recv_sem=x_recv.at[way, hop - 1, j],
            device_id={"tp": x_toward[way]},
        )

    def is_first(hop):
        return isinstance(hop, int) and hop == 1

    def m_copy(way, hop):
        source = ids_ref if is_first(hop) else ids_in.at[way, jnp.maximum(hop - 2, 0)]
        return pltpu.make_async_remote_copy(
            src_ref=source,
            dst_ref=ids_in.at[way, hop - 1],
            send_sem=m_send.at[way, hop - 1],
            recv_sem=m_recv.at[way, hop - 1],
            device_id={"st": toward[way]},
        )

    def q_copy(way, hop, j):
        source = qown.at[j] if is_first(hop) else qbuf.at[way, jnp.maximum(hop - 2, 0), j]
        return pltpu.make_async_remote_copy(
            src_ref=source,
            dst_ref=qbuf.at[way, hop - 1, j],
            send_sem=q_send.at[way, hop - 1, j],
            recv_sem=q_recv.at[way, hop - 1, j],
            device_id={"st": toward[way]},
        )

    def kv_copy(i):
        everyone = (kall, vall)[i]
        return pltpu.make_async_remote_copy(
            src_ref=everyone.at[core],
            dst_ref=everyone.at[core],
            send_sem=kv_send.at[i],
            recv_sem=kv_recv.at[i],
            device_id={"st": partner},
        )

    def r_copies(way, hop, j):
        data = pltpu.make_async_remote_copy(
            src_ref=loc.at[1 - way, hop - 1, j],
            dst_ref=rbuf.at[way, hop - 1, j],
            send_sem=r_send.at[way, hop - 1, j],
            recv_sem=r_recv.at[way, hop - 1, j],
            device_id={"st": toward[way]},
        )
        stats = pltpu.make_async_remote_copy(
            src_ref=locml.at[1 - way, hop - 1, j],
            dst_ref=rml.at[way, hop - 1, j],
            send_sem=s_send.at[way, hop - 1, j],
            recv_sem=s_recv.at[way, hop - 1, j],
            device_id={"st": toward[way]},
        )
        return data, stats

    def fill_slots(source_row, table):
        fetch = pltpu.make_async_copy(source_row, ids_s.at[table], ids_sem)
        fetch.start()
        fetch.wait()
        lowest = place * (passages * CORES)

        def step(r, state):
            found, pids, blocks = state[0], state[1 : 1 + slots], state[1 + slots :]
            offset = ids_s[table, 0, r] - lowest
            hit = jnp.logical_and(offset >= 0, offset < passages * CORES)
            here = [jnp.logical_and(hit, found == s) for s in range(slots)]
            pids = tuple(jnp.where(h, offset, p) for h, p in zip(here, pids))
            blocks = tuple(jnp.where(h, r // NPB, b) for h, b in zip(here, blocks))
            return (found + jnp.where(hit, 1, 0),) + pids + blocks

        zero = jnp.int32(0)
        state = (zero,) + (zero,) * slots + (jnp.int32(-CHUNK),) * slots
        requests = chunks * (CHUNK // BLOCK) * NPB
        state = lax.fori_loop(0, requests, step, state)
        for s in range(slots):
            pid_s[table * slots + s] = state[1 + s]
            blk_s[table * slots + s] = state[1 + slots + s]

    lanes = lax.broadcasted_iota(jnp.int32, (1, CHUNK), 1)

    def attend(query, table, j):
        base = table * slots
        keys, values, penalties = [], [], []
        for slot in range(slots):
            passage = pid_s[base + slot]
            block = blk_s[base + slot]
            keys.append(kall[passage // passages, passage % passages])
            values.append(vall[passage // passages, passage % passages])
            within = block - j * (CHUNK // BLOCK)
            penalties.append(jnp.where(lanes // BLOCK == within, 0.0, MASKED))
        scores = [
            jnp.dot(key, query, preferred_element_type=jnp.float32) * HEAD_DIM ** (-0.5) + penalty
            for key, penalty in zip(keys, penalties)
        ]
        highest = jnp.full((1, CHUNK), FLOOR, jnp.float32)
        for score in scores:
            highest = jnp.maximum(highest, jnp.max(score, 0, keepdims=True))
        exponents = [jnp.exp(score - highest) for score in scores]
        total = jnp.zeros((1, CHUNK), jnp.float32)
        for exponent in exponents:
            total = total + jnp.sum(exponent, 0, keepdims=True)
        weighted = jnp.dot(
            jnp.concatenate(values, 1),
            jnp.concatenate([e.astype(jnp.bfloat16) for e in exponents], 0),
            preferred_element_type=jnp.float32,
        )
        return weighted, highest, total

    def attend_hop(hop, ways_chunks):
        for way, j in ways_chunks:
            weighted, highest, total = attend(qbuf[way, hop - 1, j], way * far + hop - 1, j)
            loc[way, hop - 1, j] = weighted.astype(jnp.bfloat16)
            locml[way, hop - 1, j, 0:1] = highest
            locml[way, hop - 1, j, 1:2] = total

    def project(j):
        total = jnp.zeros((CHUNK, HEAD_DIM), jnp.float32)
        logits = jnp.zeros((CHUNK, wg.shape[1]), jnp.float32)
        for r in range(4):
            features = pl.ds(pl.multiple_of(x_source[r] * width, width), width)
            part = tbuf[j, r]
            total = total + jnp.dot(part, wq[features], preferred_element_type=jnp.float32)
            logits = logits + jnp.dot(part, wg[features], preferred_element_type=jnp.float32)
        qown[j] = total.T.astype(jnp.bfloat16)
        columns = lax.broadcasted_iota(jnp.int32, logits.shape, 1)
        logit = jnp.sum(jnp.where(columns == head, logits, 0.0), 1, keepdims=True)
        gate[j] = jax.nn.sigmoid(logit)

    def make_keys(part):
        count = passages // KV_PARTS
        part_rows = store[pl.ds(part * count * rows, count * rows)]
        made = jnp.dot(part_rows, wk[...], preferred_element_type=jnp.float32).astype(jnp.bfloat16)
        for i in range(count):
            kall[core, part * count + i] = made[i * rows : (i + 1) * rows]

    def make_values(part):
        count = passages // KV_PARTS
        part_rows = store[pl.ds(part * count * rows, count * rows)]
        made = jnp.dot(part_rows, wv[...], preferred_element_type=jnp.float32)
        for i in range(count):
            vall[core, part * count + i] = made[i * rows : (i + 1) * rows].T.astype(jnp.bfloat16)

    def retention(sequence):
        span = pl.ds(sequence * SEQ_LEN, SEQ_LEN)
        halfway = RET_DIM // 2

        def turned(values, scale):
            leading = values[:, :halfway].astype(jnp.float32)
            trailing = values[:, halfway:].astype(jnp.float32)
            c, s = cosines[...], sines[...]
            both = jnp.concatenate([leading * c - trailing * s, leading * s + trailing * c], 1)
            return (both * scale if scale != 1.0 else both).astype(jnp.bfloat16)

        log_gamma = jnp.float32(0.0)
        for h in range(xs):
            log_gamma = jnp.where(head == h, jnp.float32(math.log1p(-(2.0 ** (-5 - h)))), log_gamma)
        grid = (SEQ_LEN, SEQ_LEN)
        offsets = lax.broadcasted_iota(jnp.int32, grid, 0) - lax.broadcasted_iota(jnp.int32, grid, 1)
        distance = jnp.maximum(offsets, 0).astype(jnp.float32)
        decays = jnp.where(offsets >= 0, jnp.exp(log_gamma * distance), 0.0)
        scores = lax.dot_general(
            turned(rq[span], 1.0), turned(rk[span], RET_DIM ** (-0.5)),
            (((1,), (1,)), ((), ())), preferred_element_type=jnp.float32,
        )
        raw = jnp.dot((scores * decays).astype(jnp.bfloat16), rv[span], preferred_element_type=jnp.float32)
        centred = raw - jnp.mean(raw, -1, keepdims=True)
        normed = centred * lax.rsqrt(jnp.mean(centred * centred, -1, keepdims=True) + NORM_EPS)
        out_ref[span, 0:RET_DIM] = normed.astype(jnp.bfloat16)

    def merge(first, first_ml, second, second_ml):
        top = jnp.maximum(first_ml[0], second_ml[0])
        left_scale, right_scale = jnp.exp(first_ml[0] - top), jnp.exp(second_ml[0] - top)
        summed = first * left_scale + second * right_scale
        total = first_ml[1] * left_scale + second_ml[1] * right_scale
        return summed, (top, total)

    for j in range(2):
        for way in ways:
            x_copy(way, 1, j).start()
    for way in ways:
        m_copy(way, 1).start()

    def x_forward(j):
        for way in ways:
            x_copy(way, 1, j).wait_recv()
            x_copy(way, 2, j).start()
            if j + 2 < chunks:
                x_copy(way, 1, j + 2).start()

    def q_make(j):
        token_loads[j].wait()
        for way in ways:
            x_copy(way, 2, j).wait_recv()
        project(j)

    def q_send_first(j):
        for way in ways:
            q_copy(way, 1, j).start()

    def arrive(hop, j, forward=True):
        for way in ways:
            q_copy(way, hop, j).wait_recv()
            if forward:
                q_copy(way, hop + 1, j).start()

    def m_arrive(hop, forward):
        for way in ways:
            m_copy(way, hop).wait_recv()
            if forward:
                m_copy(way, hop + 1).start()
        for way in ways:
            fill_slots(ids_in.at[way, hop - 1], way * far + hop - 1)

    loads[0].wait()
    loads[1].wait()
    make_keys(0)
    x_forward(0)
    make_keys(1)
    loads[2].wait()
    x_forward(1)
    make_values(0)
    kv_copy(0).start()
    loads[3].wait()
    loads[4].wait()
    q_make(0)
    x_forward(2)
    q_send_first(0)
    make_values(1)
    q_make(1)
    x_forward(3)
    q_send_first(1)
    kv_copy(1).start()
    fill_slots(ids_ref, 2 * far)
    m_arrive(1, far > 1)
    for copy in loads[5:]:
        copy.start()
    q_make(2)
    if far > 2:
        arrive(1, 0)
    q_send_first(2)
    q_make(3)
    if far > 2:
        arrive(1, 1)
    q_send_first(3)
    for i in range(2):
        kv_copy(i).wait()

    @pl.loop(0, chunks)
    def _(j):
        weighted, highest, total = attend(qown[j], 2 * far, j)
        loc0[j] = weighted.astype(jnp.bfloat16)
        loc0ml[j, 0:1] = highest
        loc0ml[j, 1:2] = total

    def attend_all(hop):
        @pl.loop(0, chunks)
        def _(j):
            attend_hop(hop, [(0, j), (1, j)])

    if far > 2:
        arrive(1, 2)
        arrive(1, 3)
        attend_all(1)

        @pl.loop(2, far - 2)
        def _(hop):
            m_arrive(hop, True)
            for j in range(chunks):
                arrive(hop, j)
            attend_all(hop)

        hop = far - 2
        m_arrive(hop, True)
        sent = [[], []]
        for j in range(chunks):
            arrive(hop, j, False)
            for way in ways:
                for chunk in send_order[way][len(sent[way]) : chunks - 1]:
                    if chunk > j:
                        break
                    q_copy(way, hop + 1, chunk).start()
                    sent[way].append(chunk)
        attend_all(hop)
        m_arrive(far - 1, True)
    for i in range(half):
        for way in ways:
            q_copy(way, far - 1, send_order[way][i]).wait_recv()
            q_copy(way, far, send_order[way][i]).start()
    if far > 2:
        for way in ways:
            q_copy(way, far - 1, send_order[way][chunks - 1]).start()
    for i in range(half):
        attend_hop(far - 1, [(way, send_order[way][i]) for way in ways])
    for i in range(half, chunks):
        for way in ways:
            q_copy(way, far - 1, send_order[way][i]).wait_recv()
        attend_hop(far - 1, [(way, send_order[way][i]) for way in ways])
    m_arrive(far, False)
    for i in range(half):
        for way in ways:
            q_copy(way, far, far_set[way][i]).wait_recv()
        attend_hop(far, [(way, far_set[way][i]) for way in ways])

    def r_start(way, hop, j):
        for copy in r_copies(way, hop, j):
            copy.start()

    def r_merge(way, hop, j):
        for copy in r_copies(way, hop + 1, j):
            copy.wait_recv()
        summed, (top, total) = merge(
            rbuf[way, hop, j].astype(jnp.float32),
            (rml[way, hop, j, 0:1], rml[way, hop, j, 1:2]),
            loc[1 - way, hop - 1, j].astype(jnp.float32),
            (locml[1 - way, hop - 1, j, 0:1], locml[1 - way, hop - 1, j, 1:2]),
        )
        loc[1 - way, hop - 1, j] = summed.astype(jnp.bfloat16)
        locml[1 - way, hop - 1, j, 0:1] = top
        locml[1 - way, hop - 1, j, 1:2] = total

    for i in range(half):
        for way in ways:
            r_start(way, far, far_set[1 - way][i])
    for i in range(half):
        for way in ways:
            r_start(way, far - 1, far_set[way][i])

    for copy in loads[5:]:
        copy.wait()
    retention(0)
    for i in range(half):
        for way in ways:
            r_merge(way, far - 1, far_set[1 - way][i])
        for way in ways:
            r_start(way, far - 1, far_set[1 - way][i])
    retention(1)

    @pl.loop(1, far - 1)
    def _(step):
        hop = far - 1 - step
        for j in range(chunks):
            for way in ways:
                r_merge(way, hop, send_order[way][j])
            for way in ways:
                r_start(way, hop, send_order[way][j])

    done = [set(), set()]
    for i in range(chunks):
        for way in ways:
            for copy in r_copies(way, 1, send_order[way][i]):
                copy.wait_recv()
            done[way].add(send_order[way][i])

    @pl.loop(0, chunks)
    def _(j):
        summed, both = loc0[j].astype(jnp.float32), (loc0ml[j, 0:1], loc0ml[j, 1:2])
        for way in ways:
            summed, both = merge(
                summed, both, rbuf[way, 0, j].astype(jnp.float32), (rml[way, 0, j, 0:1], rml[way, 0, j, 1:2])
            )
        share = (summed / both[1]).T * gate[j]
        out_ref[pl.ds(pl.multiple_of(j * CHUNK, CHUNK), CHUNK), RET_DIM:] = share.astype(jnp.bfloat16)

    for j in range(chunks):
        for way in ways:
            for hop in (1, 2):
                x_copy(way, hop, j).wait_send()
            q_copy(way, 1, j).wait_send()
    for way in ways:
        m_copy(way, 1).wait_send()

    @pl.loop(2, far + 1)
    def _(hop):
        for way in ways:
            m_copy(way, hop).wait_send()

    @pl.loop(2, far)
    def _(hop):
        for j in range(chunks):
            for way in ways:
                q_copy(way, hop, j).wait_send()

    @pl.loop(1, far)
    def _(hop):
        for j in range(chunks):
            for way in ways:
                for copy in r_copies(way, hop, j):
                    copy.wait_send()

    for way in ways:
        for j in far_set[way]:
            q_copy(way, far, j).wait_send()
        for j in far_set[1 - way]:
            for copy in r_copies(way, far, j):
                copy.wait_send()


def body(
    tokens, ret_query, ret_key, ret_value, w_query, w_key, w_value, w_gate, store, passage_ids
):
    ring = lax.axis_size("st") // CORES
    far = ring // 2
    xs = lax.axis_size("tp")
    token_count, width = tokens.shape
    chunks = token_count // CHUNK
    passages, rows, features = store.shape
    slots = CAP * CORES
    assert xs == 4 and w_query.shape[1] == HEAD_DIM and passages % KV_PARTS == 0
    ids = jnp.pad(passage_ids.reshape(1, -1), ((0, 0), (0, 128 - passage_ids.size)))
    cosines, sines = rotary_tables()
    buffer = (2, far, chunks, HEAD_DIM, CHUNK)
    stats = (2, far, chunks, 2, CHUNK)
    flags = (2, far, chunks)
    dma = pltpu.SemaphoreType.DMA
    bf16, f32, i32 = jnp.bfloat16, jnp.float32, jnp.int32
    hbm = pl.BlockSpec(memory_space=pl.ANY)
    vmem = pl.BlockSpec(memory_space=pltpu.VMEM)
    return pl.pallas_call(
        mixer_kernel,
        out_shape=jax.ShapeDtypeStruct((token_count, RET_DIM + HEAD_DIM), bf16),
        in_specs=[vmem] + [hbm] * 11,
        out_specs=vmem,
        scratch_shapes=[
            pltpu.VMEM((chunks, 4, CHUNK, width), bf16),
            pltpu.VMEM(w_query.shape, bf16),
            pltpu.VMEM(w_key.shape, bf16),
            pltpu.VMEM(w_value.shape, bf16),
            pltpu.VMEM(w_gate.shape, bf16),
            pltpu.VMEM((passages * rows, features), bf16),
            pltpu.VMEM(ret_query.shape, bf16),
            pltpu.VMEM(ret_query.shape, bf16),
            pltpu.VMEM(ret_query.shape, bf16),
            pltpu.VMEM(cosines.shape, f32),
            pltpu.VMEM(sines.shape, f32),
            pltpu.SMEM((2 * far + 1, 1, 128), i32),
            pltpu.SMEM(((2 * far + 1) * slots,), i32),
            pltpu.SMEM(((2 * far + 1) * slots,), i32),
            pltpu.VMEM((2, far, 1, 128), i32),
            pltpu.VMEM(buffer[2:], bf16),
            pltpu.VMEM((chunks, CHUNK, 1), f32),
            pltpu.VMEM(buffer, bf16),
            pltpu.VMEM((CORES, passages, rows, HEAD_DIM), bf16),
            pltpu.VMEM((CORES, passages, HEAD_DIM, rows), bf16),
            pltpu.VMEM(buffer, bf16),
            pltpu.VMEM(stats, f32),
            pltpu.VMEM(buffer[2:], bf16),
            pltpu.VMEM(stats[2:], f32),
            pltpu.VMEM(buffer, bf16),
            pltpu.VMEM(stats, f32),
            dma((10,)),
            dma,
            dma((chunks,)),
            dma((2,)),
            dma((2,)),
            dma((2, 2, chunks)),
            dma((2, 2, chunks)),
            dma((2, far)),
            dma((2, far)),
            dma(flags),
            dma(flags),
            dma(flags),
            dma(flags),
            dma(flags),
            dma(flags),
        ],
        compiler_params=pltpu.CompilerParams(
            collective_id=0, has_side_effects=True, vmem_limit_bytes=60 * 1024 * 1024
        ),
    )(
        ids, tokens, ret_query, ret_key, ret_value, w_query, w_key, w_value, w_gate,
        store.reshape(passages * rows, features), jnp.asarray(cosines), jnp.asarray(sines),
    )


def solution(mesh):
    placed = (
        P(("grp", "st"), "tp"),
        P(("grp", "st"), "tp"),
        P(("grp", "st"), "tp"),
        P(("grp", "st"), "tp"),
        P(None, "tp"),
        P(None, "tp"),
        P(None, "tp"),
        P(),
        P("st", None, None),
        P(("grp", "st"), None),
    )
    return jax.shard_map(
        body, mesh=mesh, in_specs=placed, out_specs=P(("grp", "st"), "tp"), check_vma=False
    )
```

time: 283 us -> 229 us (0.81)
  blocking collectives: 49.2 us -> 0 us
  Pallas kernels: 183 us -> 224 us
  matrix products: 16 us -> 0 us
  between operations: 13.7 us -> 0.01 us
  other arithmetic: 13 us -> 0 us
    all_gather x1 -> x0, blocking collectives: 49.2 us -> none  [slot_tables(): ids = lax.all_gather(passage_ids.reshape(1, -1), 'st', axis=0, tiled=True)]
    pallas_call x1, Pallas kernels: 183 us -> 224 us  [body(): pl.pallas_call(mixer_kernel, out_shape=jax.ShapeDtypeStruct((token_count,...]
    dot_general x5 -> x0, matrix products: 16 us -> none  [the longest x1 4.4 us: body(): jnp.dot(store, w_key, preferred_element_type=jnp.float32)]
    convert_element_type x5 -> x0, other arithmetic: 4.81 us -> none  [the longest x1 1.78 us: retain(): key_rows.reshape(layout).astype(jnp.float32)]
    unnamed x10 -> x3, local copies, waits for them, and re-layouts: 0.98 us -> 4.59 us
  transfers between devices with their start and end apart: 1 -> 0, of which waited for: 0 -> 0; matrix products, arithmetic and copies ran while one was open for 8% -> 0% of each run, Pallas kernels for 0% -> 0%
where the time goes in v2:
time: 229 us
  Pallas kernels  224 us (98%)
  local copies, waits for them, and re-layouts  5.25 us (2%)
    pallas_call x1, Pallas kernels, body(): pl.pallas_call(mixer_kernel, out_shape=jax.ShapeDtypeStruct((token_count,...  224 us
    unnamed x3, local copies, waits for them, and re-layouts  4.59 us

profile of v2, /device:TPU:40, one launch (start us, length us, event | category | flops | bytes accessed | tf_op | source)
XLA Modules:
  0.0 229.3 jit_solution(9508410971943508390)
XLA Ops:
  0.0 0.8 copy.15
  0.8 0.1 reshape.6
  0.8 0.6 pad.4.ids_ref
  1.4 1.8 copy.16.wg_hbm
  3.2 224.0 %shard_map.118 = bf16[512,768]{1,0:T(8,128)(2,1)} custom-call(s32[1,128]{1,0:T(1,128)} %pad.4.ids_ref, bf16[512,512]{1,0:T(8,128)(2,1)} %tokens_hbm.1, bf16[512,256]{1,0:T(8,128)(2,1)} %rq_hbm.1, bf16[512,256]{1,0:T(8,128)(2,1)} %rk_hbm.1, bf16[512,256]{1,0:T(8,128)(2,1)} %rv_hbm.1, bf16[2048,512]{1,0:T(8,128)(2,1)} %wq_hbm.1, bf16[2048,512]{1,0:T(8,128)(2,1)} %wk_hbm.1, ...), custom_call_target="tpu_custom_call" | custom-call | tf_op jit(solution)/shard_map/pallas_call | solution.py:516
  227.2 2.1 copy.18

commit v3 on v2

--- a/solution.py
+++ b/solution.py
@@ -20,7 +20,8 @@
 NORM_EPS = 1e-05
 MASKED = -1e30
 FLOOR = -1e28
-KV_PARTS = 2
+PIECE = 64
+KV_PARTS = 3
 
 
 def rotary_tables():
@@ -34,7 +35,7 @@
     ids_ref, tokens_hbm, rq_hbm, rk_hbm, rv_hbm, wq_hbm, wk_hbm, wv_hbm, wg_hbm, store_hbm, cos_hbm, sin_hbm,
     out_ref,
     tbuf, wq, wk, wv, wg, store, rq, rk, rv, cosines, sines,
-    ids_s, pid_s, blk_s, ids_in, qown, gate, qbuf, kall, vall, loc, locml, loc0, loc0ml, rbuf, rml,
+    ids_s, pid_s, blk_s, ids_flat, ids_row, ids_in, qown, gate, qbuf, kall, vall, loc, locml, loc0, loc0ml, rbuf, rml,
     in_sem, ids_sem, t_sem, kv_send, kv_recv, x_send, x_recv, m_send, m_recv, q_send, q_recv,
     r_send, r_recv, s_send, s_recv,
 ):
@@ -57,6 +58,8 @@
     x_source = (head, x_left, x_right, lax.rem(head + 2, xs))
     far_set = (tuple(range(0, chunks, 2)), tuple(range(1, chunks, 2)))
     send_order = (far_set[0] + far_set[1], far_set[1] + far_set[0])
+    block_count = chunks * (CHUNK // BLOCK)
+    pieces = chunks * (CHUNK // PIECE)
     passages = kall.shape[1]
     rows = kall.shape[2]
     width = tokens_hbm.shape[1]
@@ -87,17 +90,19 @@
         pl.semaphore_signal(barrier, inc=1, device_id={"tp": device})
     pl.semaphore_wait(barrier, 5)
 
-    def x_copy(way, hop, j):
+    def x_copy(way, hop, piece):
+        j, first = divmod(piece * PIECE, CHUNK)
         if hop == 1:
-            source, target = tokens_hbm.at[pl.ds(j * CHUNK, CHUNK)], tbuf.at[j, 1 + way]
+            source = tokens_hbm.at[pl.ds(piece * PIECE, PIECE)]
+            target = tbuf.at[j, 1 + way, pl.ds(first, PIECE)]
         else:
-            part = pl.ds(way * (CHUNK // 2), CHUNK // 2)
+            part = pl.ds(first + way * (PIECE // 2), PIECE // 2)
             source, target = tbuf.at[j, 1 + way, part], tbuf.at[j, 3, part]
         return pltpu.make_async_remote_copy(
             src_ref=source,
             dst_ref=target,
-            send_sem=x_send.at[way, hop - 1, j],
-            recv_sem=x_recv.at[way, hop - 1, j],
+            send_sem=x_send.at[way, hop - 1, piece],
+            recv_sem=x_recv.at[way, hop - 1, piece],
             device_id={"tp": x_toward[way]},
         )
 
@@ -105,7 +110,7 @@
         return isinstance(hop, int) and hop == 1
 
     def m_copy(way, hop):
-        source = ids_ref if is_first(hop) else ids_in.at[way, jnp.maximum(hop - 2, 0)]
+        source = ids_row if is_first(hop) else ids_in.at[way, jnp.maximum(hop - 2, 0)]
         return pltpu.make_async_remote_copy(
             src_ref=source,
             dst_ref=ids_in.at[way, hop - 1],
@@ -151,10 +156,10 @@
         )
         return data, stats
 
-    def fill_slots(source_row, table):
-        fetch = pltpu.make_async_copy(source_row, ids_s.at[table], ids_sem)
-        fetch.start()
-        fetch.wait()
+    def fetch_ids(source_row, table):
+        return pltpu.make_async_copy(source_row, ids_s.at[table], ids_sem.at[table])
+
+    def fill_slots(table):
         lowest = place * (passages * CORES)
 
         def step(r, state):
@@ -163,13 +168,12 @@
             hit = jnp.logical_and(offset >= 0, offset < passages * CORES)
             here = [jnp.logical_and(hit, found == s) for s in range(slots)]
             pids = tuple(jnp.where(h, offset, p) for h, p in zip(here, pids))
-            blocks = tuple(jnp.where(h, r // NPB, b) for h, b in zip(here, blocks))
+            blocks = tuple(jnp.where(h, lax.rem(r, block_count), b) for h, b in zip(here, blocks))
             return (found + jnp.where(hit, 1, 0),) + pids + blocks
 
         zero = jnp.int32(0)
         state = (zero,) + (zero,) * slots + (jnp.int32(-CHUNK),) * slots
-        requests = chunks * (CHUNK // BLOCK) * NPB
-        state = lax.fori_loop(0, requests, step, state)
+        state = lax.fori_loop(0, block_count * NPB, step, state)
         for s in range(slots):
             pid_s[table * slots + s] = state[1 + s]
             blk_s[table * slots + s] = state[1 + slots + s]
@@ -213,15 +217,19 @@
 
     def project(j):
         total = jnp.zeros((CHUNK, HEAD_DIM), jnp.float32)
-        logits = jnp.zeros((CHUNK, wg.shape[1]), jnp.float32)
+        logits = jnp.zeros((wg.shape[0], CHUNK), jnp.float32)
         for r in range(4):
             features = pl.ds(pl.multiple_of(x_source[r] * width, width), width)
             part = tbuf[j, r]
             total = total + jnp.dot(part, wq[features], preferred_element_type=jnp.float32)
-            logits = logits + jnp.dot(part, wg[features], preferred_element_type=jnp.float32)
         qown[j] = total.T.astype(jnp.bfloat16)
-        columns = lax.broadcasted_iota(jnp.int32, logits.shape, 1)
-        logit = jnp.sum(jnp.where(columns == head, logits, 0.0), 1, keepdims=True)
+        for r in range(4):
+            features = pl.ds(pl.multiple_of(x_source[r] * width, width), width)
+            logits = logits + lax.dot_general(
+                wg[:, features], tbuf[j, r], (((1,), (1,)), ((), ())), preferred_element_type=jnp.float32
+            )
+        heads = lax.broadcasted_iota(jnp.int32, logits.shape, 0)
+        logit = jnp.sum(jnp.where(heads == head, logits, 0.0), 0, keepdims=True)
         gate[j] = jax.nn.sigmoid(logit)
 
     def make_keys(part):
@@ -272,23 +280,29 @@
         total = first_ml[1] * left_scale + second_ml[1] * right_scale
         return summed, (top, total)
 
-    for j in range(2):
-        for way in ways:
-            x_copy(way, 1, j).start()
-    for way in ways:
-        m_copy(way, 1).start()
-
-    def x_forward(j):
-        for way in ways:
-            x_copy(way, 1, j).wait_recv()
-            x_copy(way, 2, j).start()
-            if j + 2 < chunks:
-                x_copy(way, 1, j + 2).start()
+    for piece in range(3):
+        for way in ways:
+            x_copy(way, 1, piece).start()
+    ids_flat[...] = jnp.zeros_like(ids_flat)
+    ids_flat[:, :block_count] = ids_ref[...]
+    padded = ids_flat[...]
+    row = padded[0:1]
+    for slot in range(1, NPB):
+        row = row + pltpu.roll(padded[slot : slot + 1], slot * block_count, 1)
+    ids_row[...] = row
+
+    def x_forward(piece):
+        for way in ways:
+            x_copy(way, 1, piece).wait_recv()
+            x_copy(way, 2, piece).start()
+            if 1 <= piece < pieces - 2:
+                x_copy(way, 1, piece + 2).start()
 
     def q_make(j):
         token_loads[j].wait()
-        for way in ways:
-            x_copy(way, 2, j).wait_recv()
+        for piece in range(j * (CHUNK // PIECE), (j + 1) * (CHUNK // PIECE)):
+            for way in ways:
+                x_copy(way, 2, piece).wait_recv()
         project(j)
 
     def q_send_first(j):
@@ -306,42 +320,57 @@
             m_copy(way, hop).wait_recv()
             if forward:
                 m_copy(way, hop + 1).start()
-        for way in ways:
-            fill_slots(ids_in.at[way, hop - 1], way * far + hop - 1)
+            fetch_ids(ids_in.at[way, hop - 1], way * far + hop - 1).start()
+
+    def m_fill(hop):
+        for way in ways:
+            fetch_ids(ids_in.at[way, hop - 1], way * far + hop - 1).wait()
+            fill_slots(way * far + hop - 1)
 
     loads[0].wait()
     loads[1].wait()
     make_keys(0)
     x_forward(0)
+    for way in ways:
+        m_copy(way, 1).start()
+    fetch_ids(ids_row, 2 * far).start()
     make_keys(1)
+    x_forward(1)
+    make_keys(2)
+    x_forward(2)
     loads[2].wait()
-    x_forward(1)
     make_values(0)
-    kv_copy(0).start()
     loads[3].wait()
     loads[4].wait()
+    kv_copy(0).start()
     q_make(0)
-    x_forward(2)
+    x_forward(3)
     q_send_first(0)
     make_values(1)
+    x_forward(4)
     q_make(1)
-    x_forward(3)
+    x_forward(5)
     q_send_first(1)
-    kv_copy(1).start()
-    fill_slots(ids_ref, 2 * far)
-    m_arrive(1, far > 1)
+    make_values(2)
+    fetch_ids(ids_row, 2 * far).wait()
+    fill_slots(2 * far)
     for copy in loads[5:]:
         copy.start()
-    q_make(2)
+    m_arrive(1, far > 1)
     if far > 2:
         arrive(1, 0)
+    kv_copy(1).start()
+    x_forward(6)
+    q_make(2)
+    m_fill(1)
     q_send_first(2)
-    q_make(3)
     if far > 2:
         arrive(1, 1)
-    q_send_first(3)
+    x_forward(7)
+    q_make(3)
     for i in range(2):
         kv_copy(i).wait()
+    q_send_first(3)
 
     @pl.loop(0, chunks)
     def _(j):
@@ -365,6 +394,7 @@
             m_arrive(hop, True)
             for j in range(chunks):
                 arrive(hop, j)
+            m_fill(hop)
             attend_all(hop)
 
         hop = far - 2
@@ -378,6 +408,7 @@
                         break
                     q_copy(way, hop + 1, chunk).start()
                     sent[way].append(chunk)
+        m_fill(hop)
         attend_all(hop)
         m_arrive(far - 1, True)
     for i in range(half):
@@ -387,17 +418,7 @@
     if far > 2:
         for way in ways:
             q_copy(way, far - 1, send_order[way][chunks - 1]).start()
-    for i in range(half):
-        attend_hop(far - 1, [(way, send_order[way][i]) for way in ways])
-    for i in range(half, chunks):
-        for way in ways:
-            q_copy(way, far - 1, send_order[way][i]).wait_recv()
-        attend_hop(far - 1, [(way, send_order[way][i]) for way in ways])
-    m_arrive(far, False)
-    for i in range(half):
-        for way in ways:
-            q_copy(way, far, far_set[way][i]).wait_recv()
-        attend_hop(far, [(way, far_set[way][i]) for way in ways])
+        m_fill(far - 1)
 
     def r_start(way, hop, j):
         for copy in r_copies(way, hop, j):
@@ -417,9 +438,23 @@
         locml[1 - way, hop - 1, j, 1:2] = total
 
     for i in range(half):
+        attend_hop(far - 1, [(way, send_order[way][i]) for way in ways])
+    for way in ways:
+        q_copy(way, far - 1, send_order[way][half]).wait_recv()
+    attend_hop(far - 1, [(way, send_order[way][half]) for way in ways])
+    m_arrive(far, False)
+    m_fill(far)
+    for i in range(half):
+        for way in ways:
+            q_copy(way, far, far_set[way][i]).wait_recv()
+        attend_hop(far, [(way, far_set[way][i]) for way in ways])
         for way in ways:
             r_start(way, far, far_set[1 - way][i])
     for i in range(half):
+        if i > 0:
+            for way in ways:
+                q_copy(way, far - 1, send_order[way][half + i]).wait_recv()
+            attend_hop(far - 1, [(way, send_order[way][half + i]) for way in ways])
         for way in ways:
             r_start(way, far - 1, far_set[way][i])
 
@@ -442,30 +477,34 @@
             for way in ways:
                 r_start(way, hop, send_order[way][j])
 
-    done = [set(), set()]
-    for i in range(chunks):
-        for way in ways:
-            for copy in r_copies(way, 1, send_order[way][i]):
-                copy.wait_recv()
-            done[way].add(send_order[way][i])
-
-    @pl.loop(0, chunks)
-    def _(j):
+    def finish(j):
         summed, both = loc0[j].astype(jnp.float32), (loc0ml[j, 0:1], loc0ml[j, 1:2])
         for way in ways:
             summed, both = merge(
                 summed, both, rbuf[way, 0, j].astype(jnp.float32), (rml[way, 0, j, 0:1], rml[way, 0, j, 1:2])
             )
-        share = (summed / both[1]).T * gate[j]
-        out_ref[pl.ds(pl.multiple_of(j * CHUNK, CHUNK), CHUNK), RET_DIM:] = share.astype(jnp.bfloat16)
+        share = (summed * (gate[j] / both[1])).T
+        out_ref[j * CHUNK : (j + 1) * CHUNK, RET_DIM:] = share.astype(jnp.bfloat16)
+
+    came = [set(), set()]
+    for i in range(chunks):
+        for way in ways:
+            for copy in r_copies(way, 1, send_order[way][i]):
+                copy.wait_recv()
+        before = came[0] & came[1]
+        for way in ways:
+            came[way].add(send_order[way][i])
+        for j in sorted((came[0] & came[1]) - before):
+            finish(j)
 
     for j in range(chunks):
         for way in ways:
-            for hop in (1, 2):
-                x_copy(way, hop, j).wait_send()
             q_copy(way, 1, j).wait_send()
     for way in ways:
         m_copy(way, 1).wait_send()
+        for piece in range(pieces):
+            for hop in (1, 2):
+                x_copy(way, hop, piece).wait_send()
 
     @pl.loop(2, far + 1)
     def _(hop):
@@ -504,7 +543,7 @@
     passages, rows, features = store.shape
     slots = CAP * CORES
     assert xs == 4 and w_query.shape[1] == HEAD_DIM and passages % KV_PARTS == 0
-    ids = jnp.pad(passage_ids.reshape(1, -1), ((0, 0), (0, 128 - passage_ids.size)))
+    assert passage_ids.size <= 128
     cosines, sines = rotary_tables()
     buffer = (2, far, chunks, HEAD_DIM, CHUNK)
     stats = (2, far, chunks, 2, CHUNK)
@@ -523,7 +562,7 @@
             pltpu.VMEM(w_query.shape, bf16),
             pltpu.VMEM(w_key.shape, bf16),
             pltpu.VMEM(w_value.shape, bf16),
-            pltpu.VMEM(w_gate.shape, bf16),
+            pltpu.VMEM(w_gate.shape[::-1], bf16),
             pltpu.VMEM((passages * rows, features), bf16),
             pltpu.VMEM(ret_query.shape, bf16),
             pltpu.VMEM(ret_query.shape, bf16),
@@ -533,9 +572,11 @@
             pltpu.SMEM((2 * far + 1, 1, 128), i32),
             pltpu.SMEM(((2 * far + 1) * slots,), i32),
             pltpu.SMEM(((2 * far + 1) * slots,), i32),
+            pltpu.VMEM((NPB, 128), i32),
+            pltpu.VMEM((1, 128), i32),
             pltpu.VMEM((2, far, 1, 128), i32),
             pltpu.VMEM(buffer[2:], bf16),
-            pltpu.VMEM((chunks, CHUNK, 1), f32),
+            pltpu.VMEM((chunks, 1, CHUNK), f32),
             pltpu.VMEM(buffer, bf16),
             pltpu.VMEM((CORES, passages, rows, HEAD_DIM), bf16),
             pltpu.VMEM((CORES, passages, HEAD_DIM, rows), bf16),
@@ -546,12 +587,12 @@
             pltpu.VMEM(buffer, bf16),
             pltpu.VMEM(stats, f32),
             dma((10,)),
-            dma,
+            dma((2 * far + 1,)),
             dma((chunks,)),
             dma((2,)),
             dma((2,)),
-            dma((2, 2, chunks)),
-            dma((2, 2, chunks)),
+            dma((2, 2, token_count // PIECE)),
+            dma((2, 2, token_count // PIECE)),
             dma((2, far)),
             dma((2, far)),
             dma(flags),
@@ -565,7 +606,7 @@
             collective_id=0, has_side_effects=True, vmem_limit_bytes=60 * 1024 * 1024
         ),
     )(
-        ids, tokens, ret_query, ret_key, ret_value, w_query, w_key, w_value, w_gate,
+        passage_ids.T, tokens, ret_query, ret_key, ret_value, w_query, w_key, w_value, w_gate.T,
         store.reshape(passages * rows, features), jnp.asarray(cosines), jnp.asarray(sines),
     )
 

time: 229 us -> 216 us (0.943)
  Pallas kernels: 224 us -> 214 us
  local copies, waits for them, and re-layouts: 5.25 us -> 2.06 us
    pallas_call x1, Pallas kernels: 224 us -> 214 us  [body(): pl.pallas_call(mixer_kernel, out_shape=jax.ShapeDtypeStruct((token_count,...]
    unnamed x3 -> x1, local copies, waits for them, and re-layouts: 4.59 us -> 2.06 us
where the time goes in v3:
time: 216 us
  Pallas kernels  214 us (99%)
    pallas_call x1, Pallas kernels, body(): pl.pallas_call(mixer_kernel, out_shape=jax.ShapeDtypeStruct((token_count,...  214 us

profile of v3, /device:TPU:40, one launch (start us, length us, event | category | flops | bytes accessed | tf_op | source)
XLA Modules:
  0.0 215.6 jit_solution(4061297439899639477)
XLA Ops:
  0.0 213.5 %shard_map.118 = bf16[512,768]{1,0:T(8,128)(2,1)} custom-call(s32[4,8]{1,0:T(4,128)} %bitcast.5, bf16[512,512]{1,0:T(8,128)(2,1)} %tokens_hbm.1, bf16[512,256]{1,0:T(8,128)(2,1)} %rq_hbm.1, bf16[512,256]{1,0:T(8,128)(2,1)} %rk_hbm.1, bf16[512,256]{1,0:T(8,128)(2,1)} %rv_hbm.1, bf16[2048,512]{1,0:T(8,128)(2,1)} %wq_hbm.1, bf16[2048,512]{1,0:T(8,128)(2,1)} %wk_hbm.1, ...), custom_call_target="tpu_custom_call" | custom-call | tf_op jit(solution)/shard_map/pallas_call | solution.py:555
  213.6 2.1 copy.14

commit v4 on v3

--- a/solution.py
+++ b/solution.py
@@ -35,7 +35,7 @@
     ids_ref, tokens_hbm, rq_hbm, rk_hbm, rv_hbm, wq_hbm, wk_hbm, wv_hbm, wg_hbm, store_hbm, cos_hbm, sin_hbm,
     out_ref,
     tbuf, wq, wk, wv, wg, store, rq, rk, rv, cosines, sines,
-    ids_s, pid_s, blk_s, ids_flat, ids_row, ids_in, qown, gate, qbuf, kall, vall, loc, locml, loc0, loc0ml, rbuf, rml,
+    ids_s, pid_s, blk_s, ids_flat, ids_row, ids_in, qown, gate, qbuf, qlast_right, qlast_left, picked, kall, vall, loc, locml, loc0, loc0ml, rbuf, rml,
     in_sem, ids_sem, t_sem, kv_send, kv_recv, x_send, x_recv, m_send, m_recv, q_send, q_recv,
     r_send, r_recv, s_send, s_recv,
 ):
@@ -43,7 +43,6 @@
     ring = devices // CORES
     far = ring // 2
     chunks = qown.shape[0]
-    half = chunks // 2
     slots = CAP * CORES
     mine = lax.axis_index("st")
     place, core = mine // CORES, mine % CORES
@@ -56,14 +55,14 @@
     x_right, x_left = lax.rem(head + 1, xs), lax.rem(head + xs - 1, xs)
     x_toward = (x_right, x_left)
     x_source = (head, x_left, x_right, lax.rem(head + 2, xs))
-    far_set = (tuple(range(0, chunks, 2)), tuple(range(1, chunks, 2)))
-    send_order = (far_set[0] + far_set[1], far_set[1] + far_set[0])
     block_count = chunks * (CHUNK // BLOCK)
     pieces = chunks * (CHUNK // PIECE)
     passages = kall.shape[1]
     rows = kall.shape[2]
     width = tokens_hbm.shape[1]
     ways = range(2)
+    qlast = (qlast_right, qlast_left)
+    relay = far - 2
 
     loads = [
         pltpu.make_async_copy(source, target, in_sem.at[i])
@@ -120,10 +119,16 @@
         )
 
     def q_copy(way, hop, j):
-        source = qown.at[j] if is_first(hop) else qbuf.at[way, jnp.maximum(hop - 2, 0), j]
+        static = isinstance(hop, int)
+        if is_first(hop):
+            source = qown.at[j]
+        elif static and hop == relay + 1:
+            source = picked.at[way, j]
+        else:
+            source = qbuf.at[way, jnp.maximum(hop - 2, 0), j]
         return pltpu.make_async_remote_copy(
             src_ref=source,
-            dst_ref=qbuf.at[way, hop - 1, j],
+            dst_ref=qlast[way].at[j] if static and hop == relay else qbuf.at[way, hop - 1, j],
             send_sem=q_send.at[way, hop - 1, j],
             recv_sem=q_recv.at[way, hop - 1, j],
             device_id={"st": toward[way]},
@@ -140,15 +145,16 @@
         )
 
     def r_copies(way, hop, j):
+        passed_on = isinstance(hop, int) and hop == far - 1 and j == 0
         data = pltpu.make_async_remote_copy(
-            src_ref=loc.at[1 - way, hop - 1, j],
+            src_ref=rbuf.at[way, hop, j] if passed_on else loc.at[1 - way, hop - 1, j],
             dst_ref=rbuf.at[way, hop - 1, j],
             send_sem=r_send.at[way, hop - 1, j],
             recv_sem=r_recv.at[way, hop - 1, j],
             device_id={"st": toward[way]},
         )
         stats = pltpu.make_async_remote_copy(
-            src_ref=locml.at[1 - way, hop - 1, j],
+            src_ref=rml.at[way, hop, j] if passed_on else locml.at[1 - way, hop - 1, j],
             dst_ref=rml.at[way, hop - 1, j],
             send_sem=s_send.at[way, hop - 1, j],
             recv_sem=s_recv.at[way, hop - 1, j],
@@ -159,36 +165,42 @@
     def fetch_ids(source_row, table):
         return pltpu.make_async_copy(source_row, ids_s.at[table], ids_sem.at[table])
 
-    def fill_slots(table):
-        lowest = place * (passages * CORES)
+    def fill_slots(ids, table, target):
+        lowest = target * (passages * CORES)
 
         def step(r, state):
-            found, pids, blocks = state[0], state[1 : 1 + slots], state[1 + slots :]
-            offset = ids_s[table, 0, r] - lowest
-            hit = jnp.logical_and(offset >= 0, offset < passages * CORES)
-            here = [jnp.logical_and(hit, found == s) for s in range(slots)]
+            found, pids, blocks = state[:CORES], state[CORES : CORES + slots], state[CORES + slots :]
+            offset = ids_s[ids, 0, r] - lowest
+            hits = [
+                jnp.logical_and(offset >= c * passages, offset < (c + 1) * passages) for c in range(CORES)
+            ]
+            here = [jnp.logical_and(hits[s // CAP], found[s // CAP] == s % CAP) for s in range(slots)]
             pids = tuple(jnp.where(h, offset, p) for h, p in zip(here, pids))
             blocks = tuple(jnp.where(h, lax.rem(r, block_count), b) for h, b in zip(here, blocks))
-            return (found + jnp.where(hit, 1, 0),) + pids + blocks
+            found = tuple(f + jnp.where(h, 1, 0) for f, h in zip(found, hits))
+            return found + pids + blocks
 
         zero = jnp.int32(0)
-        state = (zero,) + (zero,) * slots + (jnp.int32(-CHUNK),) * slots
+        state = (zero,) * (CORES + slots) + (jnp.int32(-CHUNK),) * slots
         state = lax.fori_loop(0, block_count * NPB, step, state)
         for s in range(slots):
-            pid_s[table * slots + s] = state[1 + s]
-            blk_s[table * slots + s] = state[1 + slots + s]
+            pid_s[table * slots + s] = state[CORES + s]
+            blk_s[table * slots + s] = state[CORES + slots + s]
 
     lanes = lax.broadcasted_iota(jnp.int32, (1, CHUNK), 1)
 
-    def attend(query, table, j):
+    def attend(query, table, j, pair=None):
         base = table * slots
         keys, values, penalties = [], [], []
-        for slot in range(slots):
+        for slot in range(slots) if pair is None else range(pair * CAP, (pair + 1) * CAP):
             passage = pid_s[base + slot]
             block = blk_s[base + slot]
             keys.append(kall[passage // passages, passage % passages])
             values.append(vall[passage // passages, passage % passages])
-            within = block - j * (CHUNK // BLOCK)
+            if pair is None:
+                within = block - j * (CHUNK // BLOCK)
+            else:
+                within = jnp.where(block >= 0, slot % CAP, -1)
             penalties.append(jnp.where(lanes // BLOCK == within, 0.0, MASKED))
         scores = [
             jnp.dot(key, query, preferred_element_type=jnp.float32) * HEAD_DIM ** (-0.5) + penalty
@@ -210,10 +222,35 @@
 
     def attend_hop(hop, ways_chunks):
         for way, j in ways_chunks:
-            weighted, highest, total = attend(qbuf[way, hop - 1, j], way * far + hop - 1, j)
+            query = qlast[way][j] if isinstance(hop, int) and hop == relay else qbuf[way, hop - 1, j]
+            weighted, highest, total = attend(query, way * far + hop - 1, j)
             loc[way, hop - 1, j] = weighted.astype(jnp.bfloat16)
             locml[way, hop - 1, j, 0:1] = highest
             locml[way, hop - 1, j, 1:2] = total
+
+    def attend_pair(hop, way, j, pair):
+        weighted, highest, total = attend(qbuf[way, hop - 1, j], way * far + hop - 1, j, pair)
+        loc[way, hop - 1, j] = weighted.astype(jnp.bfloat16)
+        locml[way, hop - 1, j, 0:1] = highest
+        locml[way, hop - 1, j, 1:2] = total
+
+    def beyond(way, j):
+        return (2 * far + 2 + 2 * way, way) if j == 0 else (2 * far + 1 + 2 * way, j - 1)
+
+    def fill_beyond(way):
+        for away in (1, 2):
+            target = lax.rem(place + (away if way == 0 else ring - away), ring)
+            fill_slots(way * far + relay - 1, 2 * far + away + 2 * way, target)
+
+    def pick(way, j):
+        table, pair = beyond(way, j)
+        parts = []
+        for k in range(CAP):
+            block = jnp.maximum(blk_s[table * slots + pair * CAP + k], 0)
+            held = qlast[way][block // (CHUNK // BLOCK)].astype(jnp.float32)
+            turned = pltpu.roll(held, BLOCK, 1)
+            parts.append(jnp.where(block % (CHUNK // BLOCK) == k, held, turned))
+        picked[way, j] = jnp.where(lanes < BLOCK, parts[0], parts[1]).astype(jnp.bfloat16)
 
     def project(j):
         total = jnp.zeros((CHUNK, HEAD_DIM), jnp.float32)
@@ -325,7 +362,7 @@
     def m_fill(hop):
         for way in ways:
             fetch_ids(ids_in.at[way, hop - 1], way * far + hop - 1).wait()
-            fill_slots(way * far + hop - 1)
+            fill_slots(way * far + hop - 1, way * far + hop - 1, place)
 
     loads[0].wait()
     loads[1].wait()
@@ -353,19 +390,17 @@
     q_send_first(1)
     make_values(2)
     fetch_ids(ids_row, 2 * far).wait()
-    fill_slots(2 * far)
+    fill_slots(2 * far, 2 * far, place)
     for copy in loads[5:]:
         copy.start()
-    m_arrive(1, far > 1)
-    if far > 2:
-        arrive(1, 0)
+    m_arrive(1, True)
+    arrive(1, 0)
     kv_copy(1).start()
     x_forward(6)
     q_make(2)
     m_fill(1)
     q_send_first(2)
-    if far > 2:
-        arrive(1, 1)
+    arrive(1, 1)
     x_forward(7)
     q_make(3)
     for i in range(2):
@@ -384,41 +419,44 @@
         def _(j):
             attend_hop(hop, [(0, j), (1, j)])
 
-    if far > 2:
-        arrive(1, 2)
-        arrive(1, 3)
-        attend_all(1)
-
-        @pl.loop(2, far - 2)
-        def _(hop):
-            m_arrive(hop, True)
-            for j in range(chunks):
-                arrive(hop, j)
-            m_fill(hop)
-            attend_all(hop)
-
-        hop = far - 2
+    arrive(1, 2)
+    arrive(1, 3)
+    attend_all(1)
+
+    @pl.loop(2, relay - 1)
+    def _(hop):
         m_arrive(hop, True)
-        sent = [[], []]
         for j in range(chunks):
-            arrive(hop, j, False)
-            for way in ways:
-                for chunk in send_order[way][len(sent[way]) : chunks - 1]:
-                    if chunk > j:
-                        break
-                    q_copy(way, hop + 1, chunk).start()
-                    sent[way].append(chunk)
+            arrive(hop, j)
         m_fill(hop)
         attend_all(hop)
-        m_arrive(far - 1, True)
-    for i in range(half):
-        for way in ways:
-            q_copy(way, far - 1, send_order[way][i]).wait_recv()
-            q_copy(way, far, send_order[way][i]).start()
-    if far > 2:
-        for way in ways:
-            q_copy(way, far - 1, send_order[way][chunks - 1]).start()
-        m_fill(far - 1)
+
+    if relay - 1 > 1:
+        m_arrive(relay - 1, True)
+        for j in range(chunks):
+            arrive(relay - 1, j)
+        m_fill(relay - 1)
+        attend_all(relay - 1)
+
+    m_arrive(relay, True)
+    m_fill(relay)
+    for way in ways:
+        fill_beyond(way)
+    for j in range(chunks):
+        arrive(relay, j, False)
+    for j in range(2):
+        for way in ways:
+            pick(way, j)
+        for way in ways:
+            q_copy(way, relay + 1, j).start()
+    for way in ways:
+        pick(way, 2)
+    attend_hop(relay, [(way, 0) for way in ways])
+    for way in ways:
+        q_copy(way, relay + 1, 0).wait_recv()
+        q_copy(way, far, 0).start()
+    for way in ways:
+        q_copy(way, relay + 1, 2).start()
 
     def r_start(way, hop, j):
         for copy in r_copies(way, hop, j):
@@ -437,45 +475,99 @@
         locml[1 - way, hop - 1, j, 0:1] = top
         locml[1 - way, hop - 1, j, 1:2] = total
 
-    for i in range(half):
-        attend_hop(far - 1, [(way, send_order[way][i]) for way in ways])
-    for way in ways:
-        q_copy(way, far - 1, send_order[way][half]).wait_recv()
-    attend_hop(far - 1, [(way, send_order[way][half]) for way in ways])
+    def r_scatter(way, j):
+        data = [loc[1 - way, relay - 1, j].astype(jnp.float32)]
+        tops = [locml[1 - way, relay - 1, j, 0:1]]
+        totals = [locml[1 - way, relay - 1, j, 1:2]]
+        valid = [None]
+        for message in range(3):
+            table, pair = beyond(1 - way, message)
+            came = rbuf[way, relay, message].astype(jnp.float32)
+            came_top, came_total = rml[way, relay, message, 0:1], rml[way, relay, message, 1:2]
+            blocks = [blk_s[table * slots + pair * CAP + k] for k in range(CAP)]
+            for shift in range(CAP):
+                first, second = blocks[shift], blocks[1 - shift]
+                wanted = jnp.where(lanes < BLOCK, first - j * CAP, second - j * CAP - 1) == 0
+                if shift:
+                    came, came_top, came_total = (
+                        pltpu.roll(came, BLOCK, 1),
+                        pltpu.roll(came_top, BLOCK, 1),
+                        pltpu.roll(came_total, BLOCK, 1),
+                    )
+                data.append(came)
+                tops.append(jnp.where(wanted, came_top, FLOOR))
+                totals.append(came_total)
+                valid.append(wanted)
+        top = tops[0]
+        for other in tops[1:]:
+            top = jnp.maximum(top, other)
+        summed, total = None, None
+        for value, own_top, own_total, wanted in zip(data, tops, totals, valid):
+            scale = jnp.exp(own_top - top)
+            if wanted is None:
+                summed, total = value * scale, own_total * scale
+            else:
+                scale = jnp.where(wanted, scale, 0.0)
+                summed, total = summed + value * scale, total + own_total * scale
+        loc[1 - way, relay - 1, j] = summed.astype(jnp.bfloat16)
+        locml[1 - way, relay - 1, j, 0:1] = top
+        locml[1 - way, relay - 1, j, 1:2] = total
+
+    m_arrive(far - 1, True)
+
+    @pl.loop(1, chunks)
+    def _(j):
+        attend_hop(relay, [(0, j), (1, j)])
+
+    m_fill(far - 1)
+    for way in ways:
+        q_copy(way, far - 1, 1).wait_recv()
+    for way in ways:
+        attend_pair(far - 1, way, 1, 0)
     m_arrive(far, False)
     m_fill(far)
-    for i in range(half):
-        for way in ways:
-            q_copy(way, far, far_set[way][i]).wait_recv()
-        attend_hop(far, [(way, far_set[way][i]) for way in ways])
-        for way in ways:
-            r_start(way, far, far_set[1 - way][i])
-    for i in range(half):
-        if i > 0:
-            for way in ways:
-                q_copy(way, far - 1, send_order[way][half + i]).wait_recv()
-            attend_hop(far - 1, [(way, send_order[way][half + i]) for way in ways])
-        for way in ways:
-            r_start(way, far - 1, far_set[way][i])
+    for way in ways:
+        q_copy(way, far, 0).wait_recv()
+    for way in ways:
+        attend_pair(far, way, 0, way)
+    for way in ways:
+        r_start(way, far, 0)
+    for way in ways:
+        r_start(way, far - 1, 1)
+    for way in ways:
+        q_copy(way, far - 1, 2).wait_recv()
+    for way in ways:
+        attend_pair(far - 1, way, 2, 1)
+    for way in ways:
+        for copy in r_copies(way, far, 0):
+            copy.wait_recv()
+        r_start(way, far - 1, 0)
+    for way in ways:
+        r_start(way, far - 1, 2)
 
     for copy in loads[5:]:
         copy.wait()
     retention(0)
-    for i in range(half):
-        for way in ways:
-            r_merge(way, far - 1, far_set[1 - way][i])
-        for way in ways:
-            r_start(way, far - 1, far_set[1 - way][i])
     retention(1)
 
-    @pl.loop(1, far - 1)
+    for message in (1, 0, 2):
+        for way in ways:
+            for copy in r_copies(way, far - 1, message):
+                copy.wait_recv()
+    for j in range(chunks):
+        for way in ways:
+            r_scatter(way, j)
+        for way in ways:
+            r_start(way, relay, j)
+
+    @pl.loop(1, relay)
     def _(step):
-        hop = far - 1 - step
+        hop = relay - step
         for j in range(chunks):
             for way in ways:
-                r_merge(way, hop, send_order[way][j])
+                r_merge(way, hop, j)
             for way in ways:
-                r_start(way, hop, send_order[way][j])
+                r_start(way, hop, j)
 
     def finish(j):
         summed, both = loc0[j].astype(jnp.float32), (loc0ml[j, 0:1], loc0ml[j, 1:2])
@@ -486,16 +578,11 @@
         share = (summed * (gate[j] / both[1])).T
         out_ref[j * CHUNK : (j + 1) * CHUNK, RET_DIM:] = share.astype(jnp.bfloat16)
 
-    came = [set(), set()]
-    for i in range(chunks):
-        for way in ways:
-            for copy in r_copies(way, 1, send_order[way][i]):
+    for j in range(chunks):
+        for way in ways:
+            for copy in r_copies(way, 1, j):
                 copy.wait_recv()
-        before = came[0] & came[1]
-        for way in ways:
-            came[way].add(send_order[way][i])
-        for j in sorted((came[0] & came[1]) - before):
-            finish(j)
+        finish(j)
 
     for j in range(chunks):
         for way in ways:
@@ -511,13 +598,13 @@
         for way in ways:
             m_copy(way, hop).wait_send()
 
-    @pl.loop(2, far)
+    @pl.loop(2, relay)
     def _(hop):
         for j in range(chunks):
             for way in ways:
                 q_copy(way, hop, j).wait_send()
 
-    @pl.loop(1, far)
+    @pl.loop(1, relay + 1)
     def _(hop):
         for j in range(chunks):
             for way in ways:
@@ -525,11 +612,13 @@
                     copy.wait_send()
 
     for way in ways:
-        for j in far_set[way]:
-            q_copy(way, far, j).wait_send()
-        for j in far_set[1 - way]:
-            for copy in r_copies(way, far, j):
-                copy.wait_send()
+        for j in range(chunks):
+            q_copy(way, relay, j).wait_send()
+        for hop, count in ((far - 1, 3), (far, 1)):
+            for j in range(count):
+                q_copy(way, hop, j).wait_send()
+                for copy in r_copies(way, hop, j):
+                    copy.wait_send()
 
 
 def body(
@@ -542,7 +631,7 @@
     chunks = token_count // CHUNK
     passages, rows, features = store.shape
     slots = CAP * CORES
-    assert xs == 4 and w_query.shape[1] == HEAD_DIM and passages % KV_PARTS == 0
+    assert xs == 4 and far >= 4 and chunks == 4 and CHUNK == CAP * BLOCK and w_query.shape[1] == HEAD_DIM and passages % KV_PARTS == 0
     assert passage_ids.size <= 128
     cosines, sines = rotary_tables()
     buffer = (2, far, chunks, HEAD_DIM, CHUNK)
@@ -570,14 +659,17 @@
             pltpu.VMEM(cosines.shape, f32),
             pltpu.VMEM(sines.shape, f32),
             pltpu.SMEM((2 * far + 1, 1, 128), i32),
-            pltpu.SMEM(((2 * far + 1) * slots,), i32),
-            pltpu.SMEM(((2 * far + 1) * slots,), i32),
+            pltpu.SMEM(((2 * far + 5) * slots,), i32),
+            pltpu.SMEM(((2 * far + 5) * slots,), i32),
             pltpu.VMEM((NPB, 128), i32),
             pltpu.VMEM((1, 128), i32),
             pltpu.VMEM((2, far, 1, 128), i32),
             pltpu.VMEM(buffer[2:], bf16),
             pltpu.VMEM((chunks, 1, CHUNK), f32),
             pltpu.VMEM(buffer, bf16),
+            pltpu.VMEM(buffer[2:], bf16),
+            pltpu.VMEM(buffer[2:], bf16),
+            pltpu.VMEM((2, 3) + buffer[3:], bf16),
             pltpu.VMEM((CORES, passages, rows, HEAD_DIM), bf16),
             pltpu.VMEM((CORES, passages, HEAD_DIM, rows), bf16),
             pltpu.VMEM(buffer, bf16),

time: 216 us -> 211 us (0.977)
  Pallas kernels: 214 us -> 209 us
    pallas_call x1, Pallas kernels: 214 us -> 209 us  [body(): pl.pallas_call(mixer_kernel, out_shape=jax.ShapeDtypeStruct((token_count,...]
where the time goes in v4:
time: 211 us
  Pallas kernels  209 us (99%)
    pallas_call x1, Pallas kernels, body(): pl.pallas_call(mixer_kernel, out_shape=jax.ShapeDtypeStruct((token_count,...  209 us

profile of v4, /device:TPU:40, one launch (start us, length us, event | category | flops | bytes accessed | tf_op | source)
XLA Modules:
  0.0 210.8 jit_solution(13255964920210619229)
XLA Ops:
  0.0 208.8 %shard_map.118 = bf16[512,768]{1,0:T(8,128)(2,1)} custom-call(s32[4,8]{1,0:T(4,128)} %bitcast.5, bf16[512,512]{1,0:T(8,128)(2,1)} %tokens_hbm.1, bf16[512,256]{1,0:T(8,128)(2,1)} %rq_hbm.1, bf16[512,256]{1,0:T(8,128)(2,1)} %rk_hbm.1, bf16[512,256]{1,0:T(8,128)(2,1)} %rv_hbm.1, bf16[2048,512]{1,0:T(8,128)(2,1)} %wq_hbm.1, bf16[2048,512]{1,0:T(8,128)(2,1)} %wk_hbm.1, ...), custom_call_target="tpu_custom_call" | custom-call | tf_op jit(solution)/shard_map/pallas_call | solution.py:644
  208.8 2.1 copy.14

commit v5 on v4

--- a/solution.py
+++ b/solution.py
@@ -407,43 +407,65 @@
         kv_copy(i).wait()
     q_send_first(3)
 
-    @pl.loop(0, chunks)
-    def _(j):
-        weighted, highest, total = attend(qown[j], 2 * far, j)
-        loc0[j] = weighted.astype(jnp.bfloat16)
-        loc0ml[j, 0:1] = highest
-        loc0ml[j, 1:2] = total
-
-    def attend_all(hop):
+    def attend_own(first):
+        @pl.loop(first, first + 2)
+        def _(j):
+            weighted, highest, total = attend(qown[j], 2 * far, j)
+            loc0[j] = weighted.astype(jnp.bfloat16)
+            loc0ml[j, 0:1] = highest
+            loc0ml[j, 1:2] = total
+
+    def attend_both(hop, j):
+        attend_hop(hop, [(way, j) for way in ways])
+
+    def pass_hop(hop):
+        m_arrive(hop, True)
+
         @pl.loop(0, chunks)
         def _(j):
-            attend_hop(hop, [(0, j), (1, j)])
-
+            arrive(hop, j)
+            attend_both(hop - 1, j)
+
+        m_fill(hop)
+
+    attend_own(0)
     arrive(1, 2)
+    attend_own(2)
+    m_arrive(2, True)
+
+    @pl.loop(0, 2)
+    def _(j):
+        arrive(2, j, relay > 2)
+        attend_both(1, j)
+
     arrive(1, 3)
-    attend_all(1)
-
-    @pl.loop(2, relay - 1)
-    def _(hop):
-        m_arrive(hop, True)
-        for j in range(chunks):
-            arrive(hop, j)
-        m_fill(hop)
-        attend_all(hop)
-
-    if relay - 1 > 1:
-        m_arrive(relay - 1, True)
-        for j in range(chunks):
-            arrive(relay - 1, j)
-        m_fill(relay - 1)
-        attend_all(relay - 1)
-
-    m_arrive(relay, True)
-    m_fill(relay)
+
+    @pl.loop(2, chunks)
+    def _(j):
+        attend_both(1, j)
+        arrive(2, j, relay > 2)
+
+    m_fill(2)
+    if relay > 3:
+
+        @pl.loop(3, relay - 1)
+        def _(hop):
+            pass_hop(hop)
+
+        pass_hop(relay - 1)
+    if relay > 2:
+        m_arrive(relay, True)
+        m_fill(relay)
     for way in ways:
         fill_beyond(way)
-    for j in range(chunks):
-        arrive(relay, j, False)
+    if relay > 2:
+
+        @pl.loop(0, chunks - 1)
+        def _(j):
+            arrive(relay, j, False)
+            attend_both(relay - 1, j)
+
+        arrive(relay, chunks - 1, False)
     for j in range(2):
         for way in ways:
             pick(way, j)
@@ -451,7 +473,8 @@
             q_copy(way, relay + 1, j).start()
     for way in ways:
         pick(way, 2)
-    attend_hop(relay, [(way, 0) for way in ways])
+    if relay > 2:
+        attend_both(relay - 1, chunks - 1)
     for way in ways:
         q_copy(way, relay + 1, 0).wait_recv()
         q_copy(way, far, 0).start()
@@ -515,9 +538,9 @@
 
     m_arrive(far - 1, True)
 
-    @pl.loop(1, chunks)
+    @pl.loop(0, 2)
     def _(j):
-        attend_hop(relay, [(0, j), (1, j)])
+        attend_both(relay, j)
 
     m_fill(far - 1)
     for way in ways:
@@ -544,6 +567,10 @@
         r_start(way, far - 1, 0)
     for way in ways:
         r_start(way, far - 1, 2)
+
+    @pl.loop(2, chunks)
+    def _(j):
+        attend_both(relay, j)
 
     for copy in loads[5:]:
         copy.wait()

time: 211 us -> 208 us (0.986)
  Pallas kernels: 209 us -> 205 us
    pallas_call x1, Pallas kernels: 209 us -> 205 us  [body(): pl.pallas_call(mixer_kernel, out_shape=jax.ShapeDtypeStruct((token_count,...]
where the time goes in v5:
time: 208 us; the launch traced here: 207 us
  Pallas kernels  205 us (99%)
    pallas_call x1, Pallas kernels, body(): pl.pallas_call(mixer_kernel, out_shape=jax.ShapeDtypeStruct((token_count,...  205 us

profile of v5, /device:TPU:40, one launch (start us, length us, event | category | flops | bytes accessed | tf_op | source)
XLA Modules:
  0.0 207.5 jit_solution(16385412542247617183)
XLA Ops:
  0.0 205.4 %shard_map.118 = bf16[512,768]{1,0:T(8,128)(2,1)} custom-call(s32[4,8]{1,0:T(4,128)} %bitcast.5, bf16[512,512]{1,0:T(8,128)(2,1)} %tokens_hbm.1, bf16[512,256]{1,0:T(8,128)(2,1)} %rq_hbm.1, bf16[512,256]{1,0:T(8,128)(2,1)} %rk_hbm.1, bf16[512,256]{1,0:T(8,128)(2,1)} %rv_hbm.1, bf16[2048,512]{1,0:T(8,128)(2,1)} %wq_hbm.1, bf16[2048,512]{1,0:T(8,128)(2,1)} %wk_hbm.1, ...), custom_call_target="tpu_custom_call" | custom-call | tf_op jit(solution)/shard_map/pallas_call | solution.py:671
  205.4 2.1 copy.14

commit v6 on v5

--- a/solution.py
+++ b/solution.py
@@ -364,30 +364,30 @@
             fetch_ids(ids_in.at[way, hop - 1], way * far + hop - 1).wait()
             fill_slots(way * far + hop - 1, way * far + hop - 1, place)
 
+    x_forward(0)
+    for way in ways:
+        m_copy(way, 1).start()
+    fetch_ids(ids_row, 2 * far).start()
     loads[0].wait()
     loads[1].wait()
     make_keys(0)
-    x_forward(0)
-    for way in ways:
-        m_copy(way, 1).start()
-    fetch_ids(ids_row, 2 * far).start()
+    x_forward(1)
     make_keys(1)
-    x_forward(1)
+    x_forward(2)
     make_keys(2)
-    x_forward(2)
-    loads[2].wait()
-    make_values(0)
     loads[3].wait()
     loads[4].wait()
+    q_make(0)
+    q_send_first(0)
+    loads[2].wait()
     kv_copy(0).start()
-    q_make(0)
     x_forward(3)
-    q_send_first(0)
+    make_values(0)
     make_values(1)
     x_forward(4)
     q_make(1)
+    q_send_first(1)
     x_forward(5)
-    q_send_first(1)
     make_values(2)
     fetch_ids(ids_row, 2 * far).wait()
     fill_slots(2 * far, 2 * far, place)

time: 208 us -> 208 us (level)
  no operation moved by 1% of the time
where the time goes in v6:
time: 208 us
  Pallas kernels  206 us (99%)
    pallas_call x1, Pallas kernels, body(): pl.pallas_call(mixer_kernel, out_shape=jax.ShapeDtypeStruct((token_count,...  206 us

profile of v6, /device:TPU:40, one launch (start us, length us, event | category | flops | bytes accessed | tf_op | source)
XLA Modules:
  0.0 207.6 jit_solution(11798469293953942774)
XLA Ops:
  0.0 205.5 %shard_map.118 = bf16[512,768]{1,0:T(8,128)(2,1)} custom-call(s32[4,8]{1,0:T(4,128)} %bitcast.5, bf16[512,512]{1,0:T(8,128)(2,1)} %tokens_hbm.1, bf16[512,256]{1,0:T(8,128)(2,1)} %rq_hbm.1, bf16[512,256]{1,0:T(8,128)(2,1)} %rk_hbm.1, bf16[512,256]{1,0:T(8,128)(2,1)} %rv_hbm.1, bf16[2048,512]{1,0:T(8,128)(2,1)} %wq_hbm.1, bf16[2048,512]{1,0:T(8,128)(2,1)} %wk_hbm.1, ...), custom_call_target="tpu_custom_call" | custom-call | tf_op jit(solution)/shard_map/pallas_call | solution.py:671
  205.5 2.1 copy.14
